TPU v7x, 32 devices: a whole 2x2x4 slice. The times are simulated.
32 devices in a mesh: sp: 16 (over z, y, x), tp: 2 (over core).
Axes of the slice: x: 2, y: 2, z: 4, core: 2. Of those that a mesh axis runs over, the one named last changes fastest.
Arguments:
- tokens: bfloat16 [4096, 2048], P(('sp', 'tp')), may hold values from -6 to 6
- mix_gain: float32 [2048], replicated, may hold values from 0.1 to 1.9
- query_proj: bfloat16 [2048, 1536], P(None, 'tp'), may hold values from -4 to 4
- compressed_projection: bfloat16 [2048, 256], replicated, may hold values from -0.125 to 0.125
- compressed_norm_gain: float32 [256], replicated, may hold values from 0.1 to 1.9
- rope_proj: bfloat16 [2048, 64], replicated, may hold values from -0.125 to 0.125
- key_up: bfloat16 [256, 1024], P(None, 'tp'), may hold values from -4 to 4
- value_up_weight: bfloat16 [256, 1024], P(None, 'tp'), may hold values from -0.375 to 0.375
- scan_input: bfloat16 [2048, 2048], P('sp', 'tp'), may hold values from -0.125 to 0.125
- scan_gate: bfloat16 [2048, 2048], P('sp', 'tp'), may hold values from -0.125 to 0.125
- scan_write: bfloat16 [2048, 1024], P('sp', 'tp'), may hold values from -0.125 to 0.125
- scan_read: bfloat16 [2048, 1024], P('sp', 'tp'), may hold values from -0.125 to 0.125
- step_proj: bfloat16 [2048, 32], replicated, may hold values from -0.125 to 0.125
- conv_input: bfloat16 [4, 2048], P(None, 'tp'), may hold values from -3 to 3
- conv_write: bfloat16 [4, 1024], P(None, 'tp'), may hold values from -3 to 3
- conv_read: bfloat16 [4, 1024], P(None, 'tp'), may hold values from -3 to 3
- decay_log: float32 [32], P('tp'), may hold values from -16 to -2.8
- decay_offset: float32 [4096, 32], P('sp', 'tp'), may hold values from -2.2 to 0
- skip_gain: float32 [32], P('tp'), may hold values from 0.1 to 1.9
- group_gain: float32 [2048], P('tp'), may hold values from 0.1 to 1.9
Outputs:
- attended: bfloat16 [4096, 1024], P('sp', 'tp')
- scanned: bfloat16 [4096, 2048], P('sp', 'tp')
All inputs are finite; a program needn't handle non-finite values.
Results may differ from a plain program's by a relative error of at most 0.017.
The roundings to bfloat16 on the way count: a program that leaves them out, or rounds other values in their place, can miss the bound.
Values may be sent and summed in bfloat16 or wider, within the bound.
A program may use at most 128 MiB of HBM per device.

v0:
```python
import jax
import jax.numpy as jnp
from jax import lax
from jax.experimental import pallas as pl
from jax.experimental.pallas import tpu as pltpu
from jax.sharding import PartitionSpec as P

UNROTATED_WIDTH = 128
ROPE = 64
VALUE_WIDTH = 128
SSM_DIM = 64
SSM_STATE = 128


eps = 1e-06
theta = 10000.0
floor_score = -1e30


def from_behind(value, axis, steps):
    count = lax.axis_size(axis)
    initial, last = (max(0, -steps), min(count, count - steps))
    return lax.ppermute(value, axis, [(source, source + steps) for source in range(initial, last)])


def rms_scale(values, gain):
    wide = values.astype(jnp.float32)
    return wide * lax.rsqrt(jnp.mean(wide * wide, axis=-1, keepdims=True) + eps) * gain


def rotate(values, positions):
    half = values.shape[-1] // 2
    freqs = theta ** (-jnp.arange(half, dtype=jnp.float32) * 2.0 / values.shape[-1])
    angle = positions.astype(jnp.float32)[:, None] * freqs[None, :]
    cosine = jnp.cos(angle)
    sine = jnp.sin(angle)
    if values.ndim == 3:
        cosine = cosine[:, None, :]
        sine = sine[:, None, :]
    first = values[..., :half]
    second = values[..., half:]
    return jnp.concatenate(
        [first * cosine - second * sine, second * cosine + first * sine], axis=-1
    )


def short_conv(values, edge, taps):
    span = taps.shape[0]
    length = values.shape[0]
    padded = jnp.concatenate([edge, values], axis=0).astype(jnp.float32)
    result = jnp.zeros(values.shape, jnp.float32)
    for index in range(span):
        result = result + taps[index].astype(jnp.float32)[None, :] * padded[index : index + length]
    return jax.nn.silu(result).astype(jnp.bfloat16)


def local_scan(heads, steps, decays, writes, reads):
    length = decays.shape[-1]
    running = jnp.einsum(
        "grs,ls->grl",
        decays,
        jnp.tril(jnp.ones((length, length), jnp.float32)),
        precision=lax.Precision.HIGHEST,
    )
    causal = jnp.tril(jnp.ones((length, length), dtype=bool))
    spread = jnp.where(causal, running[..., :, None] - running[..., None, :], -jnp.inf)
    inner = jnp.einsum("gln,gsn->gls", reads, writes, preferred_element_type=jnp.float32)
    mixing = inner[:, None] * jnp.exp(spread) * steps[:, :, None, :]
    within = jnp.einsum(
        "grls,grsp->grlp",
        mixing.astype(jnp.bfloat16),
        heads,
        preferred_element_type=jnp.float32,
    )
    to_end = jnp.exp(running[..., -1:] - running) * steps
    weighted = (heads.astype(jnp.float32) * to_end[..., None]).astype(jnp.bfloat16)
    state = jnp.einsum(
        "grsp,gsn->grpn", weighted, writes, preferred_element_type=jnp.float32
    )
    return running, state, within


def exchange(items, plane, name, number, columns=False):
    devices, cores = lax.axis_size("sp"), lax.axis_size("tp")
    planes = devices // plane
    counts = [{"plane": plane, "line": planes, "all": devices}[item[1]] for item in items]
    amount = len(items)
    starts = [sum(counts[:i]) for i in range(amount)]
    shared = any(item[2] for item in items)

    def kernel(*refs):
        ins, outs = refs[:amount], refs[amount : 2 * amount]
        send, recv, pass_send, pass_recv, own = refs[2 * amount :]
        here, core = lax.axis_index("sp"), lax.axis_index("tp")
        across, within = here // plane, here % plane

        def place(reach, step):
            if reach == "plane":
                slot = (within + step + plane) % plane
                return across * plane + slot, slot
            if reach == "line":
                slot = (across + step + planes) % planes
                return slot * plane + within, slot
            up, along = step // plane, step % plane
            if step < 0:
                up, along = -((-step) // plane), -((-step) % plane)
            slot = (across + up + planes) % planes * plane + (within + along + plane) % plane
            return slot, slot

        barrier = pltpu.get_barrier_semaphore()
        greeted = 0
        for reach in ("plane", "line"):
            if not any(item[1] in (reach, "all") for item in items):
                continue
            size = {"plane": plane, "line": planes}[reach]
            for step in range(1, size):
                pl.semaphore_signal(
                    barrier,
                    inc=1,
                    device_id=(place(reach, step)[0], core),
                    device_id_type=pl.DeviceIdType.MESH,
                )
                greeted += 1
        if shared:
            for turn in range(1, cores):
                pl.semaphore_signal(
                    barrier,
                    inc=1,
                    device_id=(here, (core + turn) % cores),
                    device_id_type=pl.DeviceIdType.MESH,
                )
                greeted += 1
        pl.semaphore_wait(barrier, greeted)

        def target(i, slot, who):
            if columns:
                size = ins[i].shape[-1]
                return outs[i].at[:, pl.ds(pl.multiple_of(slot * size, size), size)]
            return outs[i].at[slot, who] if items[i][2] else outs[i].at[slot]

        def sent(i, step):
            goal, goal_slot = place(items[i][1], step)
            mine = place(items[i][1], 0)[1]
            if items[i][1] == "all" and step % plane and step >= plane:
                from_line = place("all", -(step // plane * plane))[1]
                return pltpu.make_async_remote_copy(
                    src_ref=target(i, from_line, core),
                    dst_ref=target(i, from_line, core),
                    send_sem=send.at[starts[i] + step],
                    recv_sem=recv.at[starts[i] + step],
                    device_id=(place("plane", step % plane)[0], core),
                    device_id_type=pl.DeviceIdType.MESH,
                )
            return pltpu.make_async_remote_copy(
                src_ref=ins[i].at[goal_slot] if items[i][3] else ins[i],
                dst_ref=target(i, mine, core),
                send_sem=send.at[starts[i] + step],
                recv_sem=recv.at[starts[i] + step],
                device_id=(goal, core),
                device_id_type=pl.DeviceIdType.MESH,
            )

        def arrived(i, step):
            slot = place(items[i][1], -step)[1]
            return pltpu.make_async_remote_copy(
                src_ref=ins[i].at[slot] if items[i][3] else ins[i],
                dst_ref=target(i, slot, core),
                send_sem=send.at[starts[i] + step],
                recv_sem=recv.at[starts[i] + step],
                device_id=(here, core),
                device_id_type=pl.DeviceIdType.MESH,
            )

        def passed(i, step, turn, outgoing):
            slot = place(items[i][1], -step)[1]
            other = (core + turn) % cores
            owner = core if outgoing else (core - turn + cores) % cores
            return pltpu.make_async_remote_copy(
                src_ref=ins[i] if step == 0 else target(i, slot, core),
                dst_ref=target(i, slot, owner),
                send_sem=pass_send.at[(starts[i] + step) * cores + turn],
                recv_sem=pass_recv.at[(starts[i] + step) * cores + turn],
                device_id=(here, other),
                device_id_type=pl.DeviceIdType.MESH,
            )

        kept = []
        for i in range(amount):
            if items[i][1] == "all":
                for up in range(1, planes):
                    sent(i, up * plane).start()
                for step in range(1, plane):
                    sent(i, step).start()
        for i in range(amount):
            if items[i][1] != "all":
                for step in range(1, counts[i]):
                    sent(i, step).start()
        for i in range(amount):
            slot = place(items[i][1], 0)[1]
            local = pltpu.make_async_copy(
                ins[i].at[slot] if items[i][3] else ins[i], target(i, slot, core), own.at[i]
            )
            local.start()
            kept.append(local)
            if items[i][2]:
                for turn in range(1, cores):
                    passed(i, 0, turn, True).start()
        for i in range(amount):
            if items[i][1] == "all":
                for up in range(1, planes):
                    arrived(i, up * plane).wait_recv()
                    for step in range(up * plane + 1, (up + 1) * plane):
                        sent(i, step).start()
                    for turn in range(1, cores):
                        passed(i, up * plane, turn, True).start()
        for i in range(amount):
            for step in range(1, counts[i]):
                if items[i][1] == "all" and step % plane == 0:
                    continue
                arrived(i, step).wait_recv()
                if items[i][2]:
                    for turn in range(1, cores):
                        passed(i, step, turn, True).start()
        for i in range(amount):
            kept[i].wait()
            for step in range(counts[i]):
                if step > 0:
                    sent(i, step).wait_send()
                if items[i][2]:
                    for turn in range(1, cores):
                        passed(i, step, turn, True).wait_send()
                        passed(i, step, turn, False).wait_recv()

    shapes = []
    for (array, reach, over, selected), count in zip(items, counts):
        lead = (count, cores) if over else (count,)
        tail = array.shape[1:] if selected else array.shape
        if columns:
            lead, tail = (), (tail[0], count * tail[1])
        shapes.append(jax.ShapeDtypeStruct(lead + tail, array.dtype))
    slots = sum(counts)
    return pl.pallas_call(
        kernel,
        out_shape=shapes,
        in_specs=[pl.BlockSpec(memory_space=pltpu.VMEM)] * amount,
        out_specs=[pl.BlockSpec(memory_space=pl.ANY)] * amount,
        scratch_shapes=[
            pltpu.SemaphoreType.DMA((slots,)),
            pltpu.SemaphoreType.DMA((slots,)),
            pltpu.SemaphoreType.DMA((slots * cores,)),
            pltpu.SemaphoreType.DMA((slots * cores,)),
            pltpu.SemaphoreType.DMA((amount,)),
        ],
        compiler_params=pltpu.CompilerParams(
            collective_id=number, has_side_effects=True, vmem_limit_bytes=16 * 1024 * 1024
        ),
        cost_estimate=pl.CostEstimate(
            flops=10**8, bytes_accessed=4 * 2**20, transcendentals=0
        ),
        name=name,
    )(*[item[0] for item in items])


def plain_exchange(items, plane):
    results = []
    for array, reach, over, selected in items:
        value = array
        if over:
            value = lax.all_gather(value, "tp")
        if reach == "plane":
            value = value if selected else value[None]
        else:
            value = lax.all_gather(value, "sp")
        results.append(value)
    return results


def gated_norm(mixed, gate, gain):
    length = mixed.shape[0]
    groups = mixed.shape[1]
    flat = mixed.reshape(length, groups, -1)
    gated = flat * jax.nn.silu(gate.astype(jnp.float32)).reshape(length, groups, -1)
    scaled = gated * lax.rsqrt(jnp.mean(gated * gated, axis=-1, keepdims=True) + eps)
    return (scaled * gain.reshape(groups, -1)[None]).reshape(length, -1).astype(jnp.bfloat16)


def attend(query, cosine, sine, keys, key_up, value_up_weight, length):
    heads = key_up.shape[1] // UNROTATED_WIDTH
    latent_width = key_up.shape[0]
    whole = UNROTATED_WIDTH + ROPE
    half = ROPE // 2
    step = 2 * length if keys.shape[0] % (2 * length) == 0 else length
    scale = whole ** (-0.5)
    contract = (((1,), (1,)), ((), ()))

    def kernel(q_ref, cos_ref, sin_ref, k_ref, ku_ref, vu_ref, out_ref, q_all, top, total, summed):
        start = lax.axis_index("sp") * length
        for h in range(heads):
            base = h * whole
            turn = q_ref[:, base + UNROTATED_WIDTH : base + whole].astype(jnp.float32)
            first, second = turn[:, :half], turn[:, half:]
            turned = jnp.concatenate(
                [
                    first * cos_ref[...] - second * sin_ref[...],
                    second * cos_ref[...] + first * sin_ref[...],
                ],
                axis=1,
            )
            q_all[h] = jnp.concatenate(
                [q_ref[:, base : base + UNROTATED_WIDTH], turned.astype(jnp.bfloat16)], axis=1
            )
        top[...] = jnp.full(top.shape, floor_score, jnp.float32)
        total[...] = jnp.zeros(total.shape, jnp.float32)
        summed[...] = jnp.zeros(summed.shape, jnp.float32)
        row = start + lax.broadcasted_iota(jnp.int32, (length, step), 0)
        column = lax.broadcasted_iota(jnp.int32, (length, step), 1)

        def visit(j, carry):
            at = pl.ds(pl.multiple_of(j * step, step), step)
            latent = k_ref[at, :latent_width]
            turned = k_ref[at, latent_width : latent_width + ROPE]
            seen = column + j * step <= row
            plain = jnp.dot(latent, ku_ref[...], preferred_element_type=jnp.float32).astype(
                jnp.bfloat16
            )
            all_values = jnp.dot(latent, vu_ref[...], preferred_element_type=jnp.float32).astype(
                jnp.bfloat16
            )
            for h in range(heads):
                values = all_values[:, h * VALUE_WIDTH : (h + 1) * VALUE_WIDTH]
                key = jnp.concatenate(
                    [plain[:, h * UNROTATED_WIDTH : (h + 1) * UNROTATED_WIDTH], turned], axis=1
                )
                scores = (
                    lax.dot_general(q_all[h], key, contract, preferred_element_type=jnp.float32)
                    * scale
                )
                scores = jnp.where(seen, scores, -jnp.inf)
                old = top[h][:, :1]
                new = jnp.maximum(old, jnp.max(scores, axis=1, keepdims=True))
                weights = jnp.exp(scores - new)
                shrink = jnp.exp(old - new)
                now = jnp.sum(weights, axis=1, keepdims=True)
                total[h] = total[h] * shrink + now
                summed[h] = summed[h] * shrink + jnp.dot(
                    weights.astype(jnp.bfloat16), values, preferred_element_type=jnp.float32
                )
                top[h] = jnp.broadcast_to(new, top.shape[1:])
            return carry

        lax.fori_loop(0, (start + length + step - 1) // step, visit, 0)
        for h in range(heads):
            out_ref[:, h * VALUE_WIDTH : (h + 1) * VALUE_WIDTH] = (
                summed[h] / total[h][:, :1]
            ).astype(jnp.bfloat16)

    return pl.pallas_call(
        kernel,
        out_shape=jax.ShapeDtypeStruct((length, heads * VALUE_WIDTH), jnp.bfloat16),
        in_specs=[pl.BlockSpec(memory_space=pltpu.VMEM)] * 6,
        out_specs=pl.BlockSpec(memory_space=pltpu.VMEM),
        scratch_shapes=[
            pltpu.VMEM((heads, length, whole), jnp.bfloat16),
            pltpu.VMEM((heads, length, 128), jnp.float32),
            pltpu.VMEM((heads, length, 128), jnp.float32),
            pltpu.VMEM((heads, length, VALUE_WIDTH), jnp.float32),
        ],
        compiler_params=pltpu.CompilerParams(vmem_limit_bytes=40 * 1024 * 1024),
        cost_estimate=pl.CostEstimate(
            flops=4 * 10**10, bytes_accessed=4 * 2**20, transcendentals=0
        ),
        name="attend",
    )(query, cosine, sine, keys, key_up, value_up_weight)


def shards(
    tokens,
    mix_gain,
    query_proj,
    compressed_projection,
    compressed_norm_gain,
    rope_proj,
    key_up,
    value_up_weight,
    scan_input,
    scan_gate,
    scan_write,
    scan_read,
    step_proj,
    conv_input,
    conv_write,
    conv_read,
    decay_log,
    decay_offset,
    skip_gain,
    group_gain,
):
    groups = scan_write.shape[1] // SSM_STATE
    devices, cores = lax.axis_size("sp"), lax.axis_size("tp")
    plane = groups if devices % groups == 0 else 1
    planes = devices // plane
    sp_index, core = lax.axis_index("sp"), lax.axis_index("tp")
    across, within = sp_index // plane, sp_index % plane
    own_groups = groups // plane
    direct = plane > 1

    def move(items, name, number, columns=False):
        if direct:
            return exchange(items, plane, name, number, columns)
        return plain_exchange(items, plane)

    depth = scan_input.shape[0]
    widths = [w.shape[1] // plane for w in (scan_input, scan_gate, scan_write, scan_read)]
    offsets = [sum(widths[:i]) for i in range(4)]
    packed = jnp.stack(
        [
            jnp.concatenate(
                [
                    w[:, n * size : (n + 1) * size]
                    for w, size in zip((scan_input, scan_gate, scan_write, scan_read), widths)
                ],
                axis=1,
            )
            for n in range(plane)
        ]
    )
    (part_weights,) = move([(packed, "plane", False, True)], "weights_in_plane", 1)
    weights = lax.all_gather(
        part_weights.reshape(plane * depth, -1),
        "sp",
        axis=0,
        tiled=True,
        axis_index_groups=[[p * plane + n for p in range(planes)] for n in range(plane)],
    )

    own_normed = rms_scale(tokens, mix_gain).astype(jnp.bfloat16)
    part = tokens.shape[0]
    length = part * cores
    latent_width = compressed_projection.shape[1]
    small = jnp.dot(
        own_normed,
        jnp.concatenate([compressed_projection, rope_proj], axis=1),
        preferred_element_type=jnp.float32,
    )
    latent = rms_scale(small[:, :latent_width], compressed_norm_gain).astype(jnp.bfloat16)
    part_positions = sp_index * length + core * part + jnp.arange(part, dtype=jnp.int32)
    key_turned = rotate(small[:, latent_width:], part_positions).astype(jnp.bfloat16)
    padding = jnp.zeros((part, -(latent_width + ROPE) % 128), jnp.bfloat16)
    own_keys = jnp.concatenate([latent, key_turned, padding], axis=1)
    all_keys, all_rows, offsets_seen = move(
        [
            (own_keys, "all", True, False),
            (own_normed, "plane", True, False),
            (decay_offset.T, "plane", False, False),
        ],
        "rows_and_keys",
        2,
    )
    all_keys = all_keys.reshape(devices * length, -1)
    all_rows = all_rows.reshape(plane * length, -1)
    edge_rows = from_behind(all_rows[plane * length - 8 :], "sp", plane)
    positions = sp_index * length + jnp.arange(length, dtype=jnp.int32)
    rows = lax.dynamic_slice_in_dim(all_rows, within * length, length, 0)
    query = jnp.dot(rows, query_proj, preferred_element_type=jnp.float32).astype(jnp.bfloat16)
    half = ROPE // 2
    freqs = theta ** (-jnp.arange(half, dtype=jnp.float32) * 2.0 / ROPE)
    angle = positions.astype(jnp.float32)[:, None] * freqs[None, :]
    attended = attend(
        query, jnp.cos(angle), jnp.sin(angle), all_keys, key_up, value_up_weight, length
    )

    def own_part(array, axis, size):
        return lax.dynamic_slice_in_dim(array, within * size, size, axis)

    local_heads = decay_log.shape[0]
    own_heads = local_heads // plane
    per_group = local_heads // groups
    step_raw = jnp.dot(
        all_rows,
        lax.dynamic_slice_in_dim(
            step_proj, core * local_heads + within * own_heads, own_heads, 1
        ),
        preferred_element_type=jnp.float32,
    )
    step_size = jax.nn.softplus(step_raw)
    own_offset = own_part(offsets_seen, 1, own_heads)
    step_values = jnp.transpose(step_size.reshape(plane, length, own_heads), (0, 2, 1))
    decay_values = (
        -jnp.exp(own_part(decay_log, 0, own_heads))[None, :, None] * step_values + own_offset
    )

    projected = jnp.dot(all_rows, weights, preferred_element_type=jnp.float32).astype(jnp.bfloat16)
    edge = jnp.dot(edge_rows, weights, preferred_element_type=jnp.float32).astype(jnp.bfloat16)
    span = conv_input.shape[0] - 1

    def convolved(i, taps):
        at = slice(offsets[i], offsets[i] + widths[i])
        return short_conv(projected[:, at], edge[8 - span :, at], own_part(taps, 1, widths[i]))

    head_conv = convolved(0, conv_input)
    gate = projected[:, offsets[1] : offsets[1] + widths[1]]
    writes = convolved(2, conv_write)
    reads = convolved(3, conv_read)
    blocks = plane * own_groups

    def by_block(values, last):
        split = values.reshape(plane, length, own_groups, last)
        return jnp.transpose(split, (0, 2, 1, 3)).reshape(blocks, length, last)

    head_values = jnp.transpose(
        head_conv.reshape(plane, length, own_groups, per_group, SSM_DIM), (0, 2, 3, 1, 4)
    ).reshape(blocks, per_group, length, SSM_DIM)
    write_values = by_block(writes, SSM_STATE)
    read_values = by_block(reads, SSM_STATE)
    running, state, mixed = local_scan(
        head_values,
        step_values.reshape(blocks, per_group, length),
        decay_values.reshape(blocks, per_group, length),
        write_values,
        read_values,
    )
    states = state.reshape(plane, own_heads, SSM_DIM, SSM_STATE)
    totals = running[..., -1].reshape(plane, own_heads)
    before, decayed = [jnp.zeros_like(states[0])], [jnp.zeros_like(totals[0])]
    for index in range(plane):
        before.append(jnp.exp(totals[index])[:, None, None] * before[-1] + states[index])
        decayed.append(totals[index] + decayed[-1])
    sent_total = jnp.pad(decayed[-1][None, :], ((0, 7), (0, 128 - own_heads)))
    seen_states, seen_totals = move(
        [
            (before[-1].reshape(-1, SSM_STATE).astype(jnp.bfloat16), "line", False, False),
            (sent_total, "line", False, False),
        ],
        "states",
        3,
    )
    seen_states = seen_states.reshape(planes, own_heads, SSM_DIM, SSM_STATE).astype(jnp.float32)
    seen_totals = seen_totals[:, 0, :own_heads]
    index = jnp.arange(planes)
    between = (index[None, :] > index[:, None]) & (index[None, :] < across)
    path = jnp.sum(jnp.where(between[:, :, None], seen_totals[None], 0.0), axis=1)
    reached = (index < across)[:, None]
    factor = jnp.where(reached, jnp.exp(path), 0.0)
    incoming = jnp.sum(seen_states * factor[:, :, None, None], axis=0)
    entered = jnp.stack(
        [
            before[k] + jnp.exp(decayed[k])[:, None, None] * incoming
            for k in range(plane)
        ]
    ).reshape(blocks, per_group, SSM_DIM, SSM_STATE)
    carried = jnp.einsum(
        "gln,grpn->grlp",
        read_values,
        entered.astype(jnp.bfloat16),
        preferred_element_type=jnp.float32,
    )
    skip = jnp.broadcast_to(
        own_part(skip_gain, 0, own_heads).reshape(1, own_groups, per_group),
        (plane, own_groups, per_group),
    ).reshape(blocks, per_group, 1, 1)
    mixed = (
        mixed
        + carried * jnp.exp(running)[..., None]
        + skip * head_values.astype(jnp.float32)
    )
    mixed = jnp.transpose(
        mixed.reshape(plane, own_groups, per_group, length, SSM_DIM), (0, 3, 1, 2, 4)
    ).reshape(plane * length, own_groups, per_group, SSM_DIM)
    scanned = gated_norm(mixed, gate, own_part(group_gain, 0, widths[0]))
    (columns,) = move(
        [(scanned.reshape(plane, length, -1), "plane", False, True)], "outputs_in_plane", 4, True
    )
    scanned = columns.reshape(length, -1)
    return (attended, scanned)


def solution(mesh):
    in_specs = (
        P(("sp", "tp"), None),
        P(),
        P(None, "tp"),
        P(),
        P(),
        P(),
        P(None, "tp"),
        P(None, "tp"),
        P("sp", "tp"),
        P("sp", "tp"),
        P("sp", "tp"),
        P("sp", "tp"),
        P(),
        P(None, "tp"),
        P(None, "tp"),
        P(None, "tp"),
        P("tp"),
        P("sp", "tp"),
        P("tp"),
        P("tp"),
    )
    out_specs = (P("sp", "tp"), P("sp", "tp"))
    return jax.shard_map(shards, mesh=mesh, in_specs=in_specs, out_specs=out_specs, check_vma=False)
```

profile of v0, /device:TPU:0, one launch (start us, length us, event | category | flops | bytes accessed | tf_op | source)
XLA Modules:
  0.0 186.1 jit_solution(546445621517097332)
XLA Ops:
  11.2 13.6 %weights_in_plane.1 = bf16[4,128,768]{2,1,0:T(8,128)(2,1)S(1)} custom-call(bf16[4,128,768]{2,1,0:T(8,128)(2,1)S(1)} %pad_maximum_fusion.refs_0_), custom_call_target="tpu_custom_call" | custom-call | flops 100000000 | bytes 4194304 | tf_op jit(solution)/shard_map/weights_in_plane/pallas_call | solution.py:242
  25.8 1.2 fusion.15
  27.0 1.0 copy.44
  28.0 1.2 fusion.17.refs_1_
  29.3 1.8 fusion.7
  31.9 50.2 %rows_and_keys.1 = (bf16[16,2,128,384]{3,2,1,0:T(8,128)(2,1)S(1)}, bf16[4,2,128,2048]{3,2,1,0:T(8,128)(2,1)S(1)}, f32[4,16,256]{2,1,0:T(8,128)S(1)}) custom-call(bf16[128,384]{1,0:T(8,128)(2,1)S(1)} %maximum_maximum_fusion.refs_0_, bf16[128,2048]{1,0:T(8,128)(2,1)S(1)} %fusion.17.refs_1_, f32[16,256]{1,0:T(8,128)S(1)} %bitcast.123), custom_call_target="tpu_custom_call" | custom-call | flops 100000000 | bytes 4194304 | tf_op jit(solution)/shard_map/rows_and_keys/pallas_call | solution.py:242
  82.1 1.7 copy-done.4
  83.8 1.9 %copy-done.1 = bf16[4,2,128,2048]{3,2,1,0:T(8,128)(2,1)} copy-done((bf16[4,2,128,2048]{3,2,1,0:T(8,128)(2,1)}, bf16[4,2,128,2048]{3,2,1,0:T(8,128)(2,1)S(1)}, u32[]{:S(2)}) %copy-start.1) | copy-done | bytes 4194328
  86.4 3.1 %collective-permute-start = (bf16[8,2048]{1,0:T(8,128)(2,1)}, bf16[8,2048]{1,0:T(8,128)(2,1)}, u32[]{:S(2)}, u32[]{:S(2)}) collective-permute-start(bf16[8,2048]{1,0:T(8,128)(2,1)} %slice.263), channel_id=1, source_target_pairs={{0,8},{2,10},{4,12},{6,14},{8,16},{10,18},{12,20},{14,22},{16,24},... | collective-permute-start | bytes 98312 | tf_op jit(solution)/shard_map/ppermute | solution.py:23
  90.0 3.4 %compare_select_fusion = f32[1024,4]{0,1:T(4,128)S(1)} fusion(bf16[1024,2048]{1,0:T(8,128)(2,1)} %bitcast.118, bf16[2048,32]{0,1:T(8,128)(2,1)} %param.32, s32[]{:T(128)S(6)} %select_n.58), kind=kOutput, calls=%fused_computation.114 | convolution fusion | flops 16801792 | bytes 4227076 | tf_op jit(solution)/shard_map/dot_general | solution.py:478
  97.2 1.3 dynamic_slice.34
  101.3 1.5 dynamic_slice.35
  102.8 1.4 fusion.74
  105.6 1.2 multiply_sine_fusion
  106.9 2.2 %convolution_convert_fusion.1.q_ref = bf16[256,768]{1,0:T(8,128)(2,1)S(1)} fusion(bf16[2048,768]{1,0:T(8,128)(2,1)S(1)} %copy-done, bf16[1024,2048]{1,0:T(8,128)(2,1)} %bitcast.119, s32[]{:T(128)S(6)} %select_n.55), kind=kOutput, calls=%fused_computation.24 | convolution fusion | flops 805502976 | bytes 4587524 | tf_op jit(solution)/shard_map/dot_general | solution.py:464
  109.1 4.4 %attend.1 = bf16[256,512]{1,0:T(8,128)(2,1)} custom-call(bf16[256,768]{1,0:T(8,128)(2,1)S(1)} %convolution_convert_fusion.1.q_ref, f32[256,32]{1,0:T(8,128)S(1)} %get-tuple-element.55.cos_ref, f32[256,32]{1,0:T(8,128)S(1)} %get-tuple-element.54.sin_ref, bf16[4096,384]{1,0:T(8,128)(2,1)S(1)} %bitcast.124, bf16[256,512]{1,0:T(8,128)(2,1)S(1)} %copy-done.6, ...), custom_call_target="tpu_custom_call" | custom-call | flops 40000000000 | bytes 4194304 | tf_op jit(solution)/shard_map/attend/pallas_call | solution.py:357
  113.6 6.7 %convolution_convert_fusion = bf16[1024,768]{1,0:T(8,128)(2,1)S(1)} fusion(bf16[1024,2048]{1,0:T(8,128)(2,1)} %bitcast.120, bf16[2048,768]{1,0:T(8,128)(2,1)} %all-gather.2.cloned.1.call-done), kind=kOutput, calls=%fused_computation.8 | convolution fusion | flops 3222011904 | bytes 8912896 | tf_op jit(solution)/shard_map/dot_general | solution.py:492
  121.1 1.3 convolution_convert_fusion.2
  123.2 1.4 multiply_convert_fusion.3
  124.6 2.8 %reshape.318 = bf16[4,256,1,4,64]{4,3,1,0,2:T(4,128)(2,1)} reshape(bf16[1024,256]{1,0:T(8,128)(2,1)} %multiply_convert_fusion.3) | data formatting | bytes 1048576 | tf_op jit(solution)/shard_map/reshape | solution.py:511
  127.4 2.2 %copy.51 = bf16[4,256,1,4,64]{1,4,3,0,2:T(8,128)(2,1)} copy(bf16[4,256,1,4,64]{4,3,1,0,2:T(4,128)(2,1)} %reshape.318) | data formatting | bytes 1048576 | tf_op jit(solution)/shard_map/reshape | solution.py:511
  129.7 1.1 multiply_convert_fusion.4
  132.1 20.3 %states.1 = (bf16[4,256,128]{2,1,0:T(8,128)(2,1)S(1)}, f32[4,8,128]{2,1,0:T(8,128)S(1)}) custom-call(bf16[256,128]{1,0:T(8,128)(2,1)S(1)} %fusion.48.refs_0_, f32[8,128]{1,0:T(8,128)S(1)} %pad.4.refs_1_), custom_call_target="tpu_custom_call" | custom-call | flops 100000000 | bytes 4194304 | tf_op jit(solution)/shard_map/states/pallas_call | solution.py:242
  153.1 1.0 maximum_convert_fusion.1
  154.1 1.0 multiply_convert_fusion.5
  155.5 1.2 fusion
  156.9 1.3 fusion.14
  158.3 2.7 %copy.59 = f32[4,256,1,4,64]{4,3,1,0,2:T(4,128)} copy(f32[4,256,1,4,64]{1,4,3,0,2:T(8,128)} %fusion.14) | data formatting | bytes 2097152 | tf_op jit(solution)/shard_map/reshape;reshape | solution.py:281
  161.0 3.2 %reshape.319 = f32[1024,256]{1,0:T(8,128)} reshape(f32[4,256,1,4,64]{4,3,1,0,2:T(4,128)} %copy.59) | data formatting | bytes 2097152 | tf_op jit(solution)/shard_map/reshape;reshape | solution.py:281
  164.2 1.8 multiply_reduce_fusion
  166.0 1.7 multiply_convert_fusion.2
  167.7 10.7 %outputs_in_plane.1 = bf16[256,1024]{1,0:T(8,128)(2,1)S(1)} custom-call(bf16[4,256,256]{2,1,0:T(8,128)(2,1)S(1)} %bitcast.122), custom_call_target="tpu_custom_call" | custom-call | flops 100000000 | bytes 4194304 | tf_op jit(solution)/shard_map/outputs_in_plane/pallas_call | solution.py:242
  (148 shorter events, 19.4 us)
Async XLA Ops:
  7.2 99.7 %copy-start = (bf16[2048,768]{1,0:T(8,128)(2,1)S(1)}, bf16[2048,768]{1,0:T(8,128)(2,1)}, u32[]{:S(2)}) copy-start(bf16[2048,768]{1,0:T(8,128)(2,1)} %param.22) | copy-start | bytes 9437188
  7.2 106.4 %all-gather.2.cloned.1.call-start = ((), (), s32[]{:S(2)}) async-start(), calls=%async_computation | async-start | bytes 3932160 | tf_op jit(solution)/shard_map/all_gather | solution.py:428
  11.0 16.1 %copy-start.16 = (bf16[2048,64]{0,1:T(8,128)(2,1)S(1)}, bf16[2048,64]{0,1:T(8,128)(2,1)}, u32[]{:S(2)}) copy-start(bf16[2048,64]{0,1:T(8,128)(2,1)} %param.25) | copy-start | bytes 786436
  11.0 17.0 %copy-start.19 = (f32[2048]{0:T(1024)S(1)}, f32[2048]{0:T(1024)}, u32[]{:S(2)}) copy-start(f32[2048]{0:T(1024)} %param.21) | copy-start | bytes 24580
  25.7 5.8 %copy-start.37 = (f32[256]{0:T(256)S(1)}, f32[256]{0:T(256)}, u32[]{:S(2)}) copy-start(f32[256]{0:T(256)} %param.24) | copy-start | bytes 3076
  25.8 6.1 %copy-start.30 = (f32[32]{0:T(128)}, f32[32]{0:T(128)S(1)}, u32[]{:S(2)}) copy-start(f32[32]{0:T(128)S(1)} %multiply_power_fusion) | copy-start | bytes 388
  25.8 6.1 %copy-start.3 = (f32[256,16]{0,1:T(8,128)S(1)}, f32[256,16]{0,1:T(8,128)}, u32[]{:S(2)}) copy-start(f32[256,16]{0,1:T(8,128)} %param.37) | copy-start | bytes 49156
  31.7 61.7 %copy-start.42 = (f32[16]{0:T(128)S(1)}, f32[16]{0:T(128)}, u32[]{:S(2)}) copy-start(f32[16]{0:T(128)} %param.36) | copy-start | bytes 196
  86.4 34.8 %collective-permute-start = (bf16[8,2048]{1,0:T(8,128)(2,1)}, bf16[8,2048]{1,0:T(8,128)(2,1)}, u32[]{:S(2)}, u32[]{:S(2)}) collective-permute-start(bf16[8,2048]{1,0:T(8,128)(2,1)} %slice.263), channel_id=1, source_target_pairs={{0,8},{2,10},{4,12},{6,14},{8,16},{10,18},{12,20},{14,22},{16,24},... | collective-permute-start | bytes 98312 | tf_op jit(solution)/shard_map/ppermute | solution.py:23
  93.5 15.5 %copy-start.6 = (bf16[256,512]{1,0:T(8,128)(2,1)S(1)}, bf16[256,512]{1,0:T(8,128)(2,1)}, u32[]{:S(2)}) copy-start(bf16[256,512]{1,0:T(8,128)(2,1)} %ku_ref.1) | copy-start | bytes 786436
  95.3 3.2 %copy-start.33 = (f32[4]{0:T(128)}, f32[4]{0:T(128)S(1)}, u32[]{:S(2)}) copy-start(f32[4]{0:T(128)S(1)} %get-tuple-element.15) | copy-start | bytes 52
  101.3 12.3 %copy-start.38 = (pred[4]{0:T(512)(128)(4,1)}, pred[4]{0:T(512)(128)(4,1)S(1)}, u32[]{:S(2)}) copy-start(pred[4]{0:T(512)(128)(4,1)S(1)} %iota_compare_fusion.3) | copy-start | bytes 16
  101.3 7.8 %copy-start.5 = (bf16[16,2,128,384]{3,2,1,0:T(8,128)(2,1)S(1)}, bf16[16,2,128,384]{3,2,1,0:T(8,128)(2,1)}, u32[]{:S(2)}) copy-start(bf16[16,2,128,384]{3,2,1,0:T(8,128)(2,1)} %copy-done.4) | copy-start | bytes 9437188
  101.3 7.8 %copy-start.7 = (bf16[256,512]{1,0:T(8,128)(2,1)S(1)}, bf16[256,512]{1,0:T(8,128)(2,1)}, u32[]{:S(2)}) copy-start(bf16[256,512]{1,0:T(8,128)(2,1)} %vu_ref.1) | copy-start | bytes 786436
  113.6 7.6 %copy-start.12 = (bf16[2048,768]{1,0:T(8,128)(2,1)S(1)}, bf16[2048,768]{1,0:T(8,128)(2,1)}, u32[]{:S(2)}) copy-start(bf16[2048,768]{1,0:T(8,128)(2,1)} %all-gather.2.cloned.1.call-done) | copy-start | bytes 9437188
  120.3 2.9 %copy-start.13 = (bf16[1024,768]{1,0:T(8,128)(2,1)}, bf16[1024,768]{1,0:T(8,128)(2,1)S(1)}, u32[]{:S(2)}) copy-start(bf16[1024,768]{1,0:T(8,128)(2,1)S(1)} %convolution_convert_fusion) | copy-start | bytes 4718596
  121.1 2.1 %copy-start.26 = (f32[1,256]{1,0:T(1,128)S(1)}, f32[1,256]{1,0:T(1,128)}, u32[]{:S(2)}) copy-start(f32[1,256]{1,0:T(1,128)} %get-tuple-element.50) | copy-start | bytes 3076
  121.1 2.1 %copy-start.27 = (f32[1,256]{1,0:T(1,128)S(1)}, f32[1,256]{1,0:T(1,128)}, u32[]{:S(2)}) copy-start(f32[1,256]{1,0:T(1,128)} %get-tuple-element.51) | copy-start | bytes 3076
  121.1 2.1 %copy-start.28 = (f32[1,256]{1,0:T(1,128)S(1)}, f32[1,256]{1,0:T(1,128)}, u32[]{:S(2)}) copy-start(f32[1,256]{1,0:T(1,128)} %get-tuple-element.52) | copy-start | bytes 3076
  121.1 2.1 %copy-start.29 = (f32[1,256]{1,0:T(1,128)S(1)}, f32[1,256]{1,0:T(1,128)}, u32[]{:S(2)}) copy-start(f32[1,256]{1,0:T(1,128)} %get-tuple-element.53) | copy-start | bytes 3076
  123.2 6.4 %copy-start.25 = (bf16[3,128]{1,0:T(4,128)(2,1)S(1)}, bf16[3,128]{1,0:T(4,128)(2,1)}, u32[]{:S(2)}) copy-start(bf16[3,128]{1,0:T(4,128)(2,1)} %get-tuple-element.48) | copy-start | bytes 2308
  129.6 2.3 %copy-start.20 = (f32[256]{0:T(256)S(1)}, f32[256]{0:T(256)}, u32[]{:S(2)}) copy-start(f32[256]{0:T(256)} %mul.567) | copy-start | bytes 3076
  129.6 2.3 %copy-start.21 = (f32[256]{0:T(256)S(1)}, f32[256]{0:T(256)}, u32[]{:S(2)}) copy-start(f32[256]{0:T(256)} %mul.564) | copy-start | bytes 3076
  129.6 2.3 %copy-start.22 = (f32[256]{0:T(256)S(1)}, f32[256]{0:T(256)}, u32[]{:S(2)}) copy-start(f32[256]{0:T(256)} %mul.561) | copy-start | bytes 3076
  129.6 22.9 %copy-start.40 = (pred[4,4]{1,0:T(4,128)(4,1)S(1)}, pred[4,4]{1,0:T(4,128)(4,1)}, u32[]{:S(2)}) copy-start(pred[4,4]{1,0:T(4,128)(4,1)} %fusion.70) | copy-start | bytes 52
  129.6 23.0 %copy-start.39 = (pred[4]{0:T(512)(128)(4,1)S(1)}, pred[4]{0:T(512)(128)(4,1)}, u32[]{:S(2)}) copy-start(pred[4]{0:T(512)(128)(4,1)} %copy-done.38) | copy-start | bytes 16
  129.7 23.4 %copy-start.24 = (bf16[3,128]{1,0:T(4,128)(2,1)S(1)}, bf16[3,128]{1,0:T(4,128)(2,1)}, u32[]{:S(2)}) copy-start(bf16[3,128]{1,0:T(4,128)(2,1)} %get-tuple-element.49) | copy-start | bytes 2308
  130.8 21.7 %copy-start.14 = (bf16[1024,128]{1,0:T(8,128)(2,1)}, bf16[1024,128]{1,0:T(8,128)(2,1)S(1)}, u32[]{:S(2)}) copy-start(bf16[1024,128]{1,0:T(8,128)(2,1)S(1)} %multiply_convert_fusion.4) | copy-start | bytes 786436
  131.9 23.5 %copy-start.18 = (f32[4,4,256]{2,1,0:T(4,128)S(1)}, f32[4,4,256]{2,1,0:T(4,128)}, u32[]{:S(2)}) copy-start(f32[4,4,256]{2,1,0:T(4,128)} %copy-done.17) | copy-start | bytes 49156
  152.8 2.3 %copy-start.15 = (bf16[1024,128]{1,0:T(8,128)(2,1)S(1)}, bf16[1024,128]{1,0:T(8,128)(2,1)}, u32[]{:S(2)}) copy-start(bf16[1024,128]{1,0:T(8,128)(2,1)} %copy-done.14) | copy-start | bytes 786436
  152.8 2.6 %copy-start.9 = (bf16[4,256,1,4,64]{1,4,3,0,2:T(8,128)(2,1)S(1)}, bf16[4,256,1,4,64]{1,4,3,0,2:T(8,128)(2,1)}, u32[]{:S(2)}) copy-start(bf16[4,256,1,4,64]{1,4,3,0,2:T(8,128)(2,1)} %copy.51) | copy-start | bytes 1572868
  161.0 5.0 %copy-start.23 = (f32[256]{0:T(256)S(1)}, f32[256]{0:T(256)}, u32[]{:S(2)}) copy-start(f32[256]{0:T(256)} %dynamic_slice.35) | copy-start | bytes 3076
  (13 other events, 15.6 us)
Sparse Core Ops, SparseCore 0:
  25.8 70.3 all-gather.1
where the time goes:
time: 187 us; the launch traced here: 186 us
  Pallas kernels  99.3 us (53%)
  local copies, waits for them, and re-layouts  31.1 us (17%)
  other arithmetic  19 us (10%)
  matrix products  18.9 us (10%)
  between operations  14.8 us (8%)
  starting transfers between devices  3.11 us (2%)
    pallas_call x4, Pallas kernels, exchange(): pl.pallas_call(kernel, out_shape=shapes, in_specs=[pl.BlockSpec(memory_sp...  94.8 us
    unnamed x88, local copies, waits for them, and re-layouts  8.21 us
    dot_general x1, matrix products, shards(): jnp.dot(all_rows, weights, preferred_element_type=jnp.float32)  6.7 us
    another operation x2, local copies, waits for them, and re-layouts, gated_norm(): flat = mixed.reshape(length, groups, -1)  5.96 us
    reshape x2, local copies, waits for them, and re-layouts, shards(): head_conv.reshape(plane, length, own_groups, per_group, SSM_DIM)  4.96 us
    pallas_call x1, Pallas kernels, attend(): pl.pallas_call(kernel, out_shape=jax.ShapeDtypeStruct((length, heads * VA...  4.45 us
  transfers between devices with their start and end apart: 2, of which 0 were waited for; matrix products, arithmetic and copies ran while one was open for 18% of the time, Pallas kernels for 29%

commit v1 on v0

--- a/solution.py
+++ b/solution.py
@@ -373,6 +373,731 @@
     )(query, cosine, sine, keys, key_up, value_up_weight)
 
 
+def fused(
+    plane,
+    tokens,
+    mix_gain,
+    query_proj,
+    compressed_projection,
+    compressed_norm_gain,
+    rope_proj,
+    key_up,
+    value_up_weight,
+    scan_input,
+    scan_gate,
+    scan_write,
+    scan_read,
+    step_proj,
+    conv_input,
+    conv_write,
+    conv_read,
+    decay_log,
+    decay_offset,
+    skip_gain,
+    group_gain,
+):
+    devices, cores = lax.axis_size("sp"), lax.axis_size("tp")
+    planes = devices // plane
+    part, width = tokens.shape
+    length = part * cores
+    depth = scan_input.shape[0]
+    kblock = depth * plane
+    hw, ww = scan_input.shape[1] // plane, scan_write.shape[1] // plane
+    lower, wide = hw + 2 * ww, 2 * hw + 2 * ww
+    bounds = ((0, lower), (lower, wide))
+    own_heads = decay_log.shape[0] // plane
+    heads = key_up.shape[1] // UNROTATED_WIDTH
+    latent_width = key_up.shape[0]
+    key_width = latent_width + 128
+    whole = UNROTATED_WIDTH + ROPE
+    half = ROPE // 2
+    scale = whole ** (-0.5)
+    span = conv_input.shape[0]
+    edge = 16
+    bf16, f32 = jnp.bfloat16, jnp.float32
+    MESH = pl.DeviceIdType.MESH
+    last_contract = (((1,), (1,)), ((), ()))
+    first_contract = (((0,), (0,)), ((), ()))
+    best = lax.Precision.HIGHEST
+    group_step = 2
+
+    def mm(a, b):
+        return jnp.dot(a, b, preferred_element_type=f32)
+
+    def kernel(
+        tok, mix, wq_hbm, comp, comp_gain, rope, ku, vu, w_in, w_gate, w_write, w_read, w_step,
+        t_in, t_write, t_read, dlog, doff, skip, ggain, freqs,
+        att_out, scan_out,
+        wq, packed, wbuf, rows, edges, keys, q_all, top, total, summed,
+        stepw, steps, osend, obuf, projf, cbuf, ybuf, runs, before, decayed, state, dsum,
+        ssend, tsend, srecv, trecv, incoming, stage,
+        wq_sem, wsend, wrecv, zsend, ksend_up, ksend_plane, ksend_core, krecv,
+        rsend, rsend_core, rrecv, o_send, o_recv, e_send, e_recv,
+        s_send, s_recv, t_send, t_recv, out_send, out_recv,
+    ):
+        here, core = lax.axis_index("sp"), lax.axis_index("tp")
+        z, n = here // plane, here % plane
+        other = cores - 1 - core
+
+        def rcopy(src, dst, ss, rs, sp, c):
+            return pltpu.make_async_remote_copy(
+                src_ref=src, dst_ref=dst, send_sem=ss, recv_sem=rs,
+                device_id=(sp, c), device_id_type=MESH,
+            )
+
+        def peer(step):
+            return z * plane + (n + step) % plane
+
+        barrier = pltpu.get_barrier_semaphore()
+        greeted = 0
+        for step in range(1, plane):
+            pl.semaphore_signal(barrier, inc=1, device_id=(peer(step), core), device_id_type=MESH)
+            greeted += 1
+        for step in range(1, planes):
+            pl.semaphore_signal(
+                barrier, inc=1, device_id=((z + step) % planes * plane + n, core),
+                device_id_type=MESH,
+            )
+            greeted += 1
+        pl.semaphore_signal(barrier, inc=1, device_id=(here, other), device_id_type=MESH)
+        greeted += 1
+        wq_copy = pltpu.make_async_copy(wq_hbm, wq, wq_sem)
+        wq_copy.start()
+
+        for m in range(plane):
+            packed[m, :, :hw] = w_in[:, m * hw : (m + 1) * hw]
+            packed[m, :, hw : hw + ww] = w_write[:, m * ww : (m + 1) * ww]
+            packed[m, :, hw + ww : lower] = w_read[:, m * ww : (m + 1) * ww]
+            packed[m, :, lower:] = w_gate[:, m * hw : (m + 1) * hw]
+        wbuf[here] = packed[n]
+        padded = jnp.concatenate(
+            [doff[...], jnp.zeros((length, 128 - doff.shape[1]), f32)], axis=1
+        )
+        turned_offsets = padded.T
+        for m in range(plane):
+            osend[m, :own_heads] = turned_offsets[m * own_heads : (m + 1) * own_heads]
+        obuf[n] = osend[n]
+
+        def normed_rows(values, gain, count):
+            mean = jnp.sum(values * values, axis=-1, keepdims=True) / count
+            return values * lax.rsqrt(mean + eps) * gain
+
+        normed = normed_rows(tok[...].astype(f32), mix[...], width).astype(bf16)
+
+        def rows_at(slot, c):
+            return pl.ds(pl.multiple_of(slot * length + c * part, part), part)
+
+        for p in range(planes):
+            rows[p, rows_at(n, core), :] = normed[:, p * kblock : (p + 1) * kblock]
+
+        def angles(start, count):
+            position = (start + lax.broadcasted_iota(jnp.int32, (count, 1), 0)).astype(f32)
+            angle = position * freqs[...]
+            return jnp.cos(angle), jnp.sin(angle)
+
+        def turn(first, second, cosine, sine):
+            return [first * cosine - second * sine, second * cosine + first * sine]
+
+        latent = normed_rows(mm(normed, comp[...]), comp_gain[...], latent_width)
+        small = mm(normed, rope[...])
+        cosine, sine = angles(here * length + core * part, part)
+        own_key = jnp.concatenate(
+            [latent]
+            + turn(small[:, :half], small[:, half:], cosine, sine)
+            + [jnp.zeros((part, key_width - latent_width - ROPE), f32)],
+            axis=1,
+        ).astype(bf16)
+        keys[here * cores + core] = own_key
+
+        pl.semaphore_wait(barrier, greeted)
+
+        def key_slot(sp, c):
+            return keys.at[sp * cores + c]
+
+        def key_copy(sp, c, ss, to_sp, to_c):
+            return rcopy(
+                key_slot(sp, c), key_slot(sp, c), ss, krecv.at[sp * cores + c], to_sp, to_c
+            )
+
+        def key_arrived(sp, c):
+            key_copy(sp, c, ksend_up.at[0], here, core).wait_recv()
+
+        def key_up_copy(d):
+            return key_copy(here, core, ksend_up.at[d], here + d * plane, core)
+
+        def key_plane_copy(d, step):
+            return key_copy(
+                here - d * plane, core, ksend_plane.at[d * plane + step], peer(step), core
+            )
+
+        def key_core_copy(sp):
+            return key_copy(sp, core, ksend_core.at[sp], here, other)
+
+        def chunk(group, index):
+            low, high = bounds[group]
+            return wbuf.at[index, :, low:high]
+
+        def w_arrived(group, index):
+            rcopy(
+                chunk(group, index), chunk(group, index), zsend.at[0, group, index],
+                wrecv.at[group, index], here, core,
+            ).wait_recv()
+
+        def w_plane_copy(group, step):
+            low, high = bounds[group]
+            goal = (n + step) % plane
+            return rcopy(
+                packed.at[goal, :, low:high], chunk(group, here), wsend.at[group, step],
+                wrecv.at[group, here], z * plane + goal, core,
+            )
+
+        def z_copy(group, index, up):
+            return rcopy(
+                chunk(group, index), chunk(group, index), zsend.at[up, group, index],
+                wrecv.at[group, index], here + (plane if up else -plane), core,
+            )
+
+        def has_next(up):
+            return z + 1 < planes if up else z > 0
+
+        def own_weights(group, steps_of):
+            for step in steps_of:
+                index = z * plane + (n - step + plane) % plane
+                if step:
+                    w_arrived(group, index)
+                for up in (0, 1):
+                    @pl.when(has_next(up))
+                    def _():
+                        z_copy(group, index, up).start()
+
+        def far_weights(group, d, forward):
+            for up in (0, 1):
+                source = z - d if up else z + d
+                exists = (source >= 0) & (source < planes)
+                gate = has_next(up) if forward else jnp.logical_not(has_next(up))
+
+                @pl.when(exists & gate)
+                def _():
+                    for q in range(plane):
+                        index = source * plane + q
+                        w_arrived(group, index)
+                        if forward:
+                            z_copy(group, index, up).start()
+
+        for d in range(1, planes):
+            @pl.when(z + d < planes)
+            def _():
+                key_up_copy(d).start()
+        for step in range(1, plane):
+            w_plane_copy(0, step).start()
+        own_weights(0, (0,))
+        for step in range(1, plane):
+            key_plane_copy(0, step).start()
+        key_core_copy(here).start()
+
+        def row_copy(slot, ss, to_sp, to_c):
+            at = rows.at[:, rows_at(slot, core), :]
+            return rcopy(at, at, ss, rrecv.at[slot * cores + core], to_sp, to_c)
+
+        def row_plane_copy(step):
+            return row_copy(n, rsend.at[step], peer(step), core)
+
+        def row_core_copy(slot):
+            return row_copy(slot, rsend_core.at[slot], here, other)
+
+        def row_arrived(slot, c):
+            at = rows.at[:, rows_at(slot, c), :]
+            rcopy(at, at, rsend.at[0], rrecv.at[slot * cores + c], here, core).wait_recv()
+
+        def offset_copy(step):
+            goal = (n + step) % plane
+            return rcopy(
+                osend.at[goal], obuf.at[n], o_send.at[step], o_recv.at[n],
+                z * plane + goal, core,
+            )
+
+        row_core_copy(n).start()
+        for step in range(1, plane):
+            offset_copy(step).start()
+
+        wq_copy.wait()
+        row_arrived(n, other)
+        own_rows = pl.ds(pl.multiple_of(n * length, length), length)
+        query = mm(rows[0, own_rows, :], wq[:kblock, :])
+        for p in range(1, planes):
+            query += mm(rows[p, own_rows, :], wq[p * kblock : (p + 1) * kblock, :])
+        query = query.astype(bf16)
+        cosine, sine = angles(here * length, length)
+        for h in range(heads):
+            base = h * whole
+            rope_part = query[:, base + UNROTATED_WIDTH : base + whole].astype(f32)
+            q_all[h] = jnp.concatenate(
+                [query[:, base : base + UNROTATED_WIDTH]]
+                + [
+                    v.astype(bf16)
+                    for v in turn(rope_part[:, :half], rope_part[:, half:], cosine, sine)
+                ],
+                axis=1,
+            )
+        top[...] = jnp.full(top.shape, floor_score, f32)
+        total[...] = jnp.zeros(total.shape, f32)
+        summed[...] = jnp.zeros(summed.shape, f32)
+
+        own_weights(0, range(1, plane))
+        for d in range(1, planes):
+            @pl.when(z >= d)
+            def _():
+                key_arrived(here - d * plane, core)
+                for step in range(1, plane):
+                    key_plane_copy(d, step).start()
+                key_core_copy(here - d * plane).start()
+        for step in range(1, plane):
+            w_plane_copy(1, step).start()
+        for step in range(1, plane):
+            row_plane_copy(step).start()
+
+        def pass_keys(d):
+            for step in range(1, plane):
+                sp = (z - d) * plane + (n + step) % plane
+                key_arrived(sp, core)
+                key_core_copy(sp).start()
+
+        def other_keys(d):
+            for q in range(plane):
+                key_arrived((z - d) * plane + q, other)
+
+        size = group_step * length
+        row = lax.broadcasted_iota(jnp.int32, (length, size), 0)
+        column = lax.broadcasted_iota(jnp.int32, (length, size), 1)
+
+        def visit(first_block, limit):
+            count = group_step * cores
+            block = keys[pl.ds(first_block * cores, count)].reshape(size, key_width)
+            lat = block[:, :latent_width]
+            turned = block[:, latent_width : latent_width + ROPE]
+            plain = mm(lat, ku[...]).astype(bf16)
+            all_values = mm(lat, vu[...]).astype(bf16)
+            if limit is not None:
+                seen = column <= row + limit
+            for h in range(heads):
+                values = all_values[:, h * VALUE_WIDTH : (h + 1) * VALUE_WIDTH]
+                key = jnp.concatenate(
+                    [plain[:, h * UNROTATED_WIDTH : (h + 1) * UNROTATED_WIDTH], turned], axis=1
+                )
+                scores = (
+                    lax.dot_general(q_all[h], key, last_contract, preferred_element_type=f32)
+                    * scale
+                )
+                if limit is not None:
+                    scores = jnp.where(seen, scores, -jnp.inf)
+                old = top[h][:, :1]
+                new = jnp.maximum(old, jnp.max(scores, axis=1, keepdims=True))
+                weights = jnp.exp(scores - new)
+                shrink = jnp.exp(old - new)
+                now = jnp.sum(weights, axis=1, keepdims=True)
+                total[h] = total[h] * shrink + now
+                summed[h] = summed[h] * shrink + mm(weights.astype(bf16), values)
+                top[h] = jnp.broadcast_to(new, top.shape[1:])
+
+        pass_keys(0)
+        other_keys(0)
+
+        def near(j, carry):
+            visit(z * plane + j * group_step, (n - j * group_step) * length)
+            return carry
+
+        lax.fori_loop(0, n // group_step + 1, near, 0)
+
+        def further(d, carry):
+            far_weights(0, d, True)
+
+            @pl.when(d == 1)
+            def _():
+                own_weights(1, range(plane))
+
+            @pl.when(z >= d)
+            def _():
+                pass_keys(d)
+                other_keys(d)
+
+                def inner(j, carry):
+                    visit((z - d) * plane + j * group_step, None)
+                    return carry
+
+                lax.fori_loop(0, plane // group_step, inner, 0)
+
+            return carry
+
+        lax.fori_loop(1, planes, further, 0)
+        for h in range(heads):
+            att_out[:, h * VALUE_WIDTH : (h + 1) * VALUE_WIDTH] = (
+                summed[h] / total[h][:, :1]
+            ).astype(bf16)
+
+        for step in range(1, plane):
+            slot = (n + step) % plane
+            row_arrived(slot, core)
+            row_core_copy(slot).start()
+        for step in range(1, plane):
+            row_arrived((n + step) % plane, other)
+        tail_at = plane * length - edge
+
+        def edge_copy():
+            return rcopy(
+                rows.at[:, tail_at : tail_at + edge, :], edges, e_send, e_recv,
+                here + plane, core,
+            )
+
+        @pl.when(z + 1 < planes)
+        def _():
+            edge_copy().start()
+
+        lane = lax.broadcasted_iota(jnp.int32, (w_step.shape[1], 128), 1)
+        which = lax.broadcasted_iota(jnp.int32, (w_step.shape[1], 128), 0)
+        first_head = (core * plane + n) * own_heads
+        chosen = ((which == lane + first_head) & (lane < own_heads)).astype(bf16)
+        stepw[...] = mm(w_step[...], chosen).astype(bf16)
+
+        def tile(k):
+            return pl.ds(pl.multiple_of(k * length, length), length)
+
+        def step_tile(k, carry):
+            raw = mm(rows[0, tile(k), :], stepw[:kblock, :])
+            for p in range(1, planes):
+                raw += mm(rows[p, tile(k), :], stepw[p * kblock : (p + 1) * kblock, :])
+            steps[k] = jnp.maximum(raw, 0.0) + jnp.log1p(jnp.exp(-jnp.abs(raw)))
+            return carry
+
+        lax.fori_loop(0, plane, step_tile, 0)
+        for d in range(1, planes):
+            far_weights(1, d, True)
+        for d in range(1, planes):
+            far_weights(0, d, False)
+
+        def project(p, values, group):
+            low, high = bounds[group]
+            block = wbuf[p * plane : (p + 1) * plane, :, low:high]
+            return mm(values, block.reshape(kblock, high - low))
+
+        @pl.when(z > 0)
+        def _():
+            rcopy(edges, edges, e_send, e_recv, here, core).wait_recv()
+            first = project(0, edges[0], 0)
+            for p in range(1, planes):
+                first += project(p, edges[p], 0)
+            projf[:edge, :] = first.astype(bf16).astype(f32)
+
+        @pl.when(z == 0)
+        def _():
+            projf[:edge, :] = jnp.zeros((edge, lower), f32)
+
+        def project_tile(k, carry):
+            out = project(0, rows[0, tile(k), :], 0)
+            for p in range(1, planes):
+                out += project(p, rows[p, tile(k), :], 0)
+            at = pl.ds(pl.multiple_of(k * length + edge, edge), length)
+            projf[at, :] = out.astype(bf16).astype(f32)
+            return carry
+
+        lax.fori_loop(0, plane, project_tile, 0)
+
+        taps = jnp.concatenate(
+            [
+                t_in[:, pl.ds(pl.multiple_of(n * hw, hw), hw)],
+                t_write[:, pl.ds(pl.multiple_of(n * ww, ww), ww)],
+                t_read[:, pl.ds(pl.multiple_of(n * ww, ww), ww)],
+            ],
+            axis=1,
+        ).astype(f32)
+
+        def conv_tile(k, carry):
+            base = pl.ds(pl.multiple_of(k * length, length), length + edge)
+            for low in range(0, lower, 128):
+                at = slice(low, low + 128)
+                values = projf[base, at]
+                result = jnp.zeros((length, 128), f32)
+                for i in range(span):
+                    shift = edge - span + 1 + i
+                    result = result + taps[i : i + 1, at] * values[shift : shift + length]
+                cbuf[tile(k), at] = (result * jax.nn.sigmoid(result)).astype(bf16)
+            return carry
+
+        lax.fori_loop(0, plane, conv_tile, 0)
+
+        for step in range(1, plane):
+            slot = (n - step + plane) % plane
+            rcopy(
+                obuf.at[slot], obuf.at[slot], o_send.at[0], o_recv.at[slot], here, core
+            ).wait_recv()
+        lane_row = lax.broadcasted_iota(jnp.int32, (1, 128), 1)
+        rate = jnp.zeros((1, 128), f32)
+        for h in range(own_heads):
+            rate = jnp.where(lane_row == h, dlog[n * own_heads + h], rate)
+        rate = -jnp.exp(rate)
+        causal = lax.broadcasted_iota(jnp.int32, (length, length), 0) >= lax.broadcasted_iota(
+            jnp.int32, (length, length), 1
+        )
+        tri = causal.astype(f32)
+
+        def per_lane(columns):
+            return jnp.concatenate(
+                [
+                    jnp.broadcast_to(columns[:, h : h + 1], (columns.shape[0], SSM_DIM))
+                    for h in range(own_heads)
+                ],
+                axis=1,
+            )
+
+        def per_row(values):
+            return jnp.concatenate(
+                [
+                    jnp.broadcast_to(values[:, h : h + 1], (SSM_DIM, SSM_STATE))
+                    for h in range(own_heads)
+                ],
+                axis=0,
+            )
+
+        state[...] = jnp.zeros(state.shape, f32)
+        dsum[...] = jnp.zeros(dsum.shape, f32)
+
+        def scan_tile(k, carry):
+            step_col = steps[k]
+            off_col = jnp.concatenate(
+                [obuf[k], jnp.zeros((128 - obuf.shape[1], length), f32)], axis=0
+            ).T
+            decay = jnp.where(lane_row < own_heads, rate * step_col + off_col, 0.0)
+            running = jnp.dot(tri, decay, precision=best, preferred_element_type=f32)
+            runs[k] = running
+            run_row, step_row = running.T, step_col.T
+            x = cbuf[tile(k), :hw]
+            w = cbuf[tile(k), hw : hw + ww]
+            r = cbuf[tile(k), hw + ww : lower]
+            inner = lax.dot_general(r, w, last_contract, preferred_element_type=f32)
+            for h in range(own_heads):
+                at = slice(h * SSM_DIM, (h + 1) * SSM_DIM)
+                spread = jnp.where(
+                    causal, running[:, h : h + 1] - run_row[h : h + 1, :], -jnp.inf
+                )
+                mixing = inner * jnp.exp(spread) * step_row[h : h + 1, :]
+                ybuf[tile(k), at] = (
+                    mm(mixing.astype(bf16), x[:, at])
+                    + skip[n * own_heads + h] * x[:, at].astype(f32)
+                )
+            last = running[length - 1 : length, :]
+            to_end = jnp.exp(last - running) * step_col
+            weighted = (x.astype(f32) * per_lane(to_end)).astype(bf16)
+            update = lax.dot_general(weighted, w, first_contract, preferred_element_type=f32)
+            before[k] = state[...]
+            decayed[k] = dsum[...]
+            state[...] = per_row(jnp.exp(last)) * state[...] + update
+            dsum[...] = dsum[...] + last
+            return carry
+
+        lax.fori_loop(0, plane, scan_tile, 0)
+
+        ssend[...] = state[...].astype(bf16)
+        tsend[...] = dsum[...]
+
+        def state_copies(d):
+            to = here + d * plane
+            return (
+                rcopy(ssend, srecv.at[z], s_send.at[d], s_recv.at[z], to, core),
+                rcopy(tsend, trecv.at[z], t_send.at[d], t_recv.at[z], to, core),
+            )
+
+        for d in range(1, planes):
+            @pl.when(z + d < planes)
+            def _():
+                for copy in state_copies(d):
+                    copy.start()
+
+        for d in range(1, planes):
+            far_weights(1, d, False)
+        incoming[...] = jnp.zeros(incoming.shape, f32)
+        for p in range(planes - 1):
+            @pl.when(p < z)
+            def _():
+                rcopy(
+                    ssend, srecv.at[p], s_send.at[0], s_recv.at[p], here, core
+                ).wait_recv()
+                rcopy(
+                    tsend, trecv.at[p], t_send.at[0], t_recv.at[p], here, core
+                ).wait_recv()
+                incoming[...] = per_row(jnp.exp(trecv[p][:1])) * incoming[...] + srecv[
+                    p
+                ].astype(f32)
+
+        own_columns = pl.ds(pl.multiple_of(n * hw, hw), hw)
+        gain = ggain[:, own_columns]
+
+        def out_copy(k):
+            return rcopy(
+                stage.at[k], scan_out.at[:, own_columns], out_send.at[k], out_recv.at[n],
+                z * plane + k, core,
+            )
+
+        def finish(i, carry):
+            k = (n + 1 + i) % plane
+            gate = project(0, rows[0, tile(k), :], 1)
+            for p in range(1, planes):
+                gate += project(p, rows[p, tile(k), :], 1)
+            gate = gate.astype(bf16).astype(f32)
+            entered = (
+                before[k] + per_row(jnp.exp(decayed[k][:1])) * incoming[...]
+            ).astype(bf16)
+            carried = lax.dot_general(
+                cbuf[tile(k), hw + ww : lower], entered, last_contract,
+                preferred_element_type=f32,
+            )
+            mixed = ybuf[tile(k), :] + carried * per_lane(jnp.exp(runs[k]))
+            gated = mixed * (gate * jax.nn.sigmoid(gate))
+            out = normed_rows(gated, gain, hw).astype(bf16)
+            stage[k] = out
+
+            @pl.when(k != n)
+            def _():
+                out_copy(k).start()
+
+            @pl.when(k == n)
+            def _():
+                scan_out[:, own_columns] = out
+
+            return carry
+
+        lax.fori_loop(0, plane, finish, 0)
+        for step in range(1, plane):
+            slot = (n + step) % plane
+            at = scan_out.at[:, pl.ds(pl.multiple_of(slot * hw, hw), hw)]
+            rcopy(stage.at[0], at, out_send.at[0], out_recv.at[slot], here, core).wait_recv()
+
+        for d in range(1, planes):
+            @pl.when(z + d < planes)
+            def _():
+                key_up_copy(d).wait_send()
+                for copy in state_copies(d):
+                    copy.wait_send()
+        for d in range(planes):
+            @pl.when(z >= d)
+            def _():
+                for step in range(1, plane):
+                    key_plane_copy(d, step).wait_send()
+                for q in range(plane):
+                    key_core_copy((z - d) * plane + q).wait_send()
+        for step in range(1, plane):
+            for group in (0, 1):
+                w_plane_copy(group, step).wait_send()
+            row_plane_copy(step).wait_send()
+            offset_copy(step).wait_send()
+            out_copy((n + step) % plane).wait_send()
+        for slot in range(plane):
+            row_core_copy(slot).wait_send()
+
+        @pl.when(z + 1 < planes)
+        def _():
+            edge_copy().wait_send()
+
+        for up in (0, 1):
+            for p in range(planes):
+                @pl.when(((p <= z) if up else (p >= z)) & has_next(up))
+                def _():
+                    for q in range(plane):
+                        for group in (0, 1):
+                            z_copy(group, p * plane + q, up).wait_send()
+
+    vmem = pl.BlockSpec(memory_space=pltpu.VMEM)
+    smem = pl.BlockSpec(memory_space=pltpu.SMEM)
+    hbm = pl.BlockSpec(memory_space=pltpu.HBM)
+    freqs = theta ** (-jnp.arange(half, dtype=f32) * 2.0 / ROPE)
+    dma = pltpu.SemaphoreType.DMA
+    positions = plane * length
+    return pl.pallas_call(
+        kernel,
+        out_shape=(
+            jax.ShapeDtypeStruct((length, heads * VALUE_WIDTH), bf16),
+            jax.ShapeDtypeStruct((length, scan_input.shape[1]), bf16),
+        ),
+        in_specs=[vmem, vmem, hbm] + [vmem] * 13 + [smem, vmem, smem, vmem, vmem],
+        out_specs=(vmem, vmem),
+        scratch_shapes=[
+            pltpu.VMEM(query_proj.shape, bf16),
+            pltpu.VMEM((plane, depth, wide), bf16),
+            pltpu.VMEM((devices, depth, wide), bf16),
+            pltpu.VMEM((planes, positions, kblock), bf16),
+            pltpu.VMEM((planes, edge, kblock), bf16),
+            pltpu.VMEM((devices * cores, part, key_width), bf16),
+            pltpu.VMEM((heads, length, whole), bf16),
+            pltpu.VMEM((heads, length, 128), f32),
+            pltpu.VMEM((heads, length, 128), f32),
+            pltpu.VMEM((heads, length, VALUE_WIDTH), f32),
+            pltpu.VMEM((width, 128), bf16),
+            pltpu.VMEM((plane, length, 128), f32),
+            pltpu.VMEM((plane, 8, length), f32),
+            pltpu.VMEM((plane, 8, length), f32),
+            pltpu.VMEM((edge + positions, lower), f32),
+            pltpu.VMEM((positions, lower), bf16),
+            pltpu.VMEM((positions, hw), f32),
+            pltpu.VMEM((plane, length, 128), f32),
+            pltpu.VMEM((plane, own_heads * SSM_DIM, SSM_STATE), f32),
+            pltpu.VMEM((plane, 8, 128), f32),
+            pltpu.VMEM((own_heads * SSM_DIM, SSM_STATE), f32),
+            pltpu.VMEM((8, 128), f32),
+            pltpu.VMEM((own_heads * SSM_DIM, SSM_STATE), bf16),
+            pltpu.VMEM((8, 128), f32),
+            pltpu.VMEM((planes, own_heads * SSM_DIM, SSM_STATE), bf16),
+            pltpu.VMEM((planes, 8, 128), f32),
+            pltpu.VMEM((own_heads * SSM_DIM, SSM_STATE), f32),
+            pltpu.VMEM((plane, length, hw), bf16),
+            dma,
+            dma((2, plane)),
+            dma((2, devices)),
+            dma((2, 2, devices)),
+            dma((planes,)),
+            dma((planes * plane,)),
+            dma((devices,)),
+            dma((devices * cores,)),
+            dma((plane,)),
+            dma((plane,)),
+            dma((plane * cores,)),
+            dma((plane,)),
+            dma((plane,)),
+            dma,
+            dma,
+            dma((planes,)),
+            dma((planes,)),
+            dma((planes,)),
+            dma((planes,)),
+            dma((plane,)),
+            dma((plane,)),
+        ],
+        compiler_params=pltpu.CompilerParams(
+            collective_id=1, has_side_effects=True, vmem_limit_bytes=60 * 1024 * 1024
+        ),
+        name="fused",
+    )(
+        tokens,
+        mix_gain[None, :],
+        query_proj,
+        compressed_projection,
+        compressed_norm_gain[None, :],
+        rope_proj,
+        key_up,
+        value_up_weight,
+        scan_input,
+        scan_gate,
+        scan_write,
+        scan_read,
+        step_proj,
+        conv_input,
+        conv_write,
+        conv_read,
+        decay_log,
+        decay_offset,
+        skip_gain,
+        group_gain[None, :],
+        freqs[None, :],
+    )
+
+
 def shards(
     tokens,
     mix_gain,
@@ -403,6 +1128,30 @@
     across, within = sp_index // plane, sp_index % plane
     own_groups = groups // plane
     direct = plane > 1
+    if direct and cores == 2 and own_groups == 1 and plane % 2 == 0 and planes > 1:
+        return fused(
+            plane,
+            tokens,
+            mix_gain,
+            query_proj,
+            compressed_projection,
+            compressed_norm_gain,
+            rope_proj,
+            key_up,
+            value_up_weight,
+            scan_input,
+            scan_gate,
+            scan_write,
+            scan_read,
+            step_proj,
+            conv_input,
+            conv_write,
+            conv_read,
+            decay_log,
+            decay_offset,
+            skip_gain,
+            group_gain,
+        )
 
     def move(items, name, number, columns=False):
         if direct:

time: 187 us -> 100 us (0.53)
  the two profiles are of different devices: /device:TPU:0 before, /device:TPU:28 now
where the time goes in v1:
time: 100 us; the launch traced here: 99 us
  Pallas kernels  88.9 us (89%)
  local copies, waits for them, and re-layouts  8.86 us (9%)
    pallas_call x1, Pallas kernels, fused(): pl.pallas_call(kernel, out_shape=(jax.ShapeDtypeStruct((length, heads * V...  88.9 us
    unnamed x5, local copies, waits for them, and re-layouts  8.86 us

profile of v1, /device:TPU:28, one launch (start us, length us, event | category | flops | bytes accessed | tf_op | source)
XLA Modules:
  0.0 99.0 jit_solution(10408357929884101103)
XLA Ops:
  0.6 0.5 multiply_power_fusion.freqs
  1.2 1.5 %copy.24.doff = f32[256,16]{1,0:T(8,128)} copy(f32[256,16]{0,1:T(8,128)} %param.37) | data formatting | bytes 32768 | tf_op args[17]
  2.6 2.0 %copy.22.rope = bf16[2048,64]{1,0:T(8,128)(2,1)} copy(bf16[2048,64]{0,1:T(8,128)(2,1)} %param.25) | data formatting | bytes 524288 | tf_op args[5]
  4.6 1.9 %copy.23.w_step = bf16[2048,32]{1,0:T(8,128)(2,1)} copy(bf16[2048,32]{0,1:T(8,128)(2,1)} %param.32) | data formatting | bytes 262144 | tf_op args[12]
  6.5 88.9 %fused.1 = (bf16[256,512]{1,0:T(8,128)(2,1)}, bf16[256,1024]{1,0:T(8,128)(2,1)}) custom-call(bf16[128,2048]{1,0:T(8,128)(2,1)} %tok.1, f32[1,2048]{1,0:T(1,128)} %bitcast.3, bf16[2048,768]{1,0:T(8,128)(2,1)} %wq_hbm.1, bf16[2048,256]{1,0:T(8,128)(2,1)} %comp.1, f32[1,256]{1,0:T(1,128)} %bitcast.5, bf16[2048,64]{1,0:T(8,128)(2,1)} %copy.22.rope, ...), custom_call_target="tpu_custom_call" | custom-call | tf_op jit(solution)/shard_map/fused/pallas_call | solution.py:1013
  95.4 1.7 %copy.27 = bf16[256,512]{1,0:T(8,128)(2,1)} copy(bf16[256,512]{1,0:T(8,128)(2,1)} %get-tuple-element.4) | data formatting | bytes 524288
  97.1 1.9 %copy.28 = bf16[256,1024]{1,0:T(8,128)(2,1)} copy(bf16[256,1024]{1,0:T(8,128)(2,1)} %get-tuple-element.5) | data formatting | bytes 1048576

commit v2 on v1

--- a/solution.py
+++ b/solution.py
@@ -1,5 +1,6 @@
 import jax
 import jax.numpy as jnp
+import numpy as np
 from jax import lax
 from jax.experimental import pallas as pl
 from jax.experimental.pallas import tpu as pltpu
@@ -408,7 +409,7 @@
     own_heads = decay_log.shape[0] // plane
     heads = key_up.shape[1] // UNROTATED_WIDTH
     latent_width = key_up.shape[0]
-    key_width = latent_width + 128
+    key_rows = (latent_width + ROPE) * part // 128
     whole = UNROTATED_WIDTH + ROPE
     half = ROPE // 2
     scale = whole ** (-0.5)
@@ -425,19 +426,37 @@
         return jnp.dot(a, b, preferred_element_type=f32)
 
     def kernel(
-        tok, mix, wq_hbm, comp, comp_gain, rope, ku, vu, w_in, w_gate, w_write, w_read, w_step,
-        t_in, t_write, t_read, dlog, doff, skip, ggain, freqs,
-        att_out, scan_out,
-        wq, packed, wbuf, rows, edges, keys, q_all, top, total, summed,
-        stepw, steps, osend, obuf, projf, cbuf, ybuf, runs, before, decayed, state, dsum,
-        ssend, tsend, srecv, trecv, incoming, stage,
-        wq_sem, wsend, wrecv, zsend, ksend_up, ksend_plane, ksend_core, krecv,
-        rsend, rsend_core, rrecv, o_send, o_recv, e_send, e_recv,
-        s_send, s_recv, t_send, t_recv, out_send, out_recv,
+        *refs
     ):
+        sources, (dlog, skip) = refs[:loaded], refs[loaded : loaded + 2]
+        att_out, scan_out = refs[loaded + 2 : loaded + 4]
+        targets = refs[loaded + 4 : 2 * loaded + 4]
+        (
+            w_in, w_write, w_read, w_gate, tok, mix, comp, comp_gain, rope, freqs, wq, ku, vu,
+            doff, w_step, t_in, t_write, t_read, ggain,
+        ) = targets
+        (
+            load_sem, packed, wbuf, rows, keys, q_all, top, total, summed, stepw, steps, osend,
+            obuf, projf, gatef, cbuf, ybuf, runs, before, decayed, state, dsum, ssend, tsend,
+            srecv, trecv, incoming, stage, wsend, wrecv, zsend, ksend_up, ksend_plane,
+            ksend_core, krecv, rsend, rsend_core, rrecv, rdiag_send,
+            rdiag_recv, o_send, o_recv, e_send, e_recv, s_send, s_recv, t_send, t_recv,
+            out_send, out_recv,
+        ) = refs[2 * loaded + 4 :]
         here, core = lax.axis_index("sp"), lax.axis_index("tp")
         z, n = here // plane, here % plane
         other = cores - 1 - core
+        beside, above, across = n + 1 - 2 * (n % 2), (n + 2) % plane, plane - 1 - n
+        at_end = (z == 0) | (z == planes - 1)
+        nearest = (z + planes - 1) // planes
+        farthest = planes - 1 - z
+
+        loads = [
+            pltpu.make_async_copy(source, target, load_sem.at[i])
+            for i, (source, target) in enumerate(zip(sources, targets))
+        ]
+        for load in loads:
+            load.start()
 
         def rcopy(src, dst, ss, rs, sp, c):
             return pltpu.make_async_remote_copy(
@@ -461,8 +480,8 @@
             greeted += 1
         pl.semaphore_signal(barrier, inc=1, device_id=(here, other), device_id_type=MESH)
         greeted += 1
-        wq_copy = pltpu.make_async_copy(wq_hbm, wq, wq_sem)
-        wq_copy.start()
+        for load in loads[:4]:
+            load.wait()
 
         for m in range(plane):
             packed[m, :, :hw] = w_in[:, m * hw : (m + 1) * hw]
@@ -470,44 +489,6 @@
             packed[m, :, hw + ww : lower] = w_read[:, m * ww : (m + 1) * ww]
             packed[m, :, lower:] = w_gate[:, m * hw : (m + 1) * hw]
         wbuf[here] = packed[n]
-        padded = jnp.concatenate(
-            [doff[...], jnp.zeros((length, 128 - doff.shape[1]), f32)], axis=1
-        )
-        turned_offsets = padded.T
-        for m in range(plane):
-            osend[m, :own_heads] = turned_offsets[m * own_heads : (m + 1) * own_heads]
-        obuf[n] = osend[n]
-
-        def normed_rows(values, gain, count):
-            mean = jnp.sum(values * values, axis=-1, keepdims=True) / count
-            return values * lax.rsqrt(mean + eps) * gain
-
-        normed = normed_rows(tok[...].astype(f32), mix[...], width).astype(bf16)
-
-        def rows_at(slot, c):
-            return pl.ds(pl.multiple_of(slot * length + c * part, part), part)
-
-        for p in range(planes):
-            rows[p, rows_at(n, core), :] = normed[:, p * kblock : (p + 1) * kblock]
-
-        def angles(start, count):
-            position = (start + lax.broadcasted_iota(jnp.int32, (count, 1), 0)).astype(f32)
-            angle = position * freqs[...]
-            return jnp.cos(angle), jnp.sin(angle)
-
-        def turn(first, second, cosine, sine):
-            return [first * cosine - second * sine, second * cosine + first * sine]
-
-        latent = normed_rows(mm(normed, comp[...]), comp_gain[...], latent_width)
-        small = mm(normed, rope[...])
-        cosine, sine = angles(here * length + core * part, part)
-        own_key = jnp.concatenate(
-            [latent]
-            + turn(small[:, :half], small[:, half:], cosine, sine)
-            + [jnp.zeros((part, key_width - latent_width - ROPE), f32)],
-            axis=1,
-        ).astype(bf16)
-        keys[here * cores + core] = own_key
 
         pl.semaphore_wait(barrier, greeted)
 
@@ -525,6 +506,8 @@
         def key_up_copy(d):
             return key_copy(here, core, ksend_up.at[d], here + d * plane, core)
 
+        sides = (beside, above)
+
         def key_plane_copy(d, step):
             return key_copy(
                 here - d * plane, core, ksend_plane.at[d * plane + step], peer(step), core
@@ -532,6 +515,8 @@
 
         def key_core_copy(sp):
             return key_copy(sp, core, ksend_core.at[sp], here, other)
+
+        sides = (beside, above)
 
         def chunk(group, index):
             low, high = bounds[group]
@@ -584,14 +569,52 @@
                         if forward:
                             z_copy(group, index, up).start()
 
+        for step in range(1, plane):
+            w_plane_copy(0, step).start()
+        own_weights(0, (0,))
+
+        for load in loads[4:10]:
+            load.wait()
+        def normed_rows(values, gain, count):
+            mean = jnp.sum(values * values, axis=-1, keepdims=True) / count
+            return values * lax.rsqrt(mean + eps) * gain
+
+        normed = normed_rows(tok[...].astype(f32), mix[...], width).astype(bf16)
+
+        def rows_at(slot, c):
+            return pl.ds(pl.multiple_of(slot * length + c * part, part), part)
+
+        for p in range(planes):
+            rows[p, rows_at(n, core), :] = normed[:, p * kblock : (p + 1) * kblock]
+
+        def angles(start, count):
+            position = (start + lax.broadcasted_iota(jnp.int32, (count, 1), 0)).astype(f32)
+            angle = position * freqs[...]
+            return jnp.cos(angle), jnp.sin(angle)
+
+        def turn(first, second, cosine, sine):
+            return [first * cosine - second * sine, second * cosine + first * sine]
+
+        latent = normed_rows(mm(normed, comp[...]), comp_gain[...], latent_width)
+        small = lax.dot_general(normed, rope[...], last_contract, preferred_element_type=f32)
+        cosine, sine = angles(here * length + core * part, part)
+        own_slot = here * cores + core
+        for low in range(0, latent_width, 128):
+            keys[own_slot, low * part // 128 : (low + 128) * part // 128] = latent[
+                :, low : low + 128
+            ].astype(bf16)
+        turned_key = jnp.concatenate(
+            turn(small[:, :half], small[:, half:], cosine, sine), axis=1
+        ).astype(bf16)
+        keys[own_slot, latent_width * part // 128 :] = jnp.concatenate(
+            [turned_key[: part // 2], turned_key[part // 2 :]], axis=1
+        )
+
         for d in range(1, planes):
             @pl.when(z + d < planes)
             def _():
                 key_up_copy(d).start()
         for step in range(1, plane):
-            w_plane_copy(0, step).start()
-        own_weights(0, (0,))
-        for step in range(1, plane):
             key_plane_copy(0, step).start()
         key_core_copy(here).start()
 
@@ -599,8 +622,16 @@
             at = rows.at[:, rows_at(slot, core), :]
             return rcopy(at, at, ss, rrecv.at[slot * cores + core], to_sp, to_c)
 
-        def row_plane_copy(step):
-            return row_copy(n, rsend.at[step], peer(step), core)
+        def row_plane_copy(side):
+            return row_copy(n, rsend.at[side], z * plane + sides[side], core)
+
+        def row_part(slot, side, to_sp):
+            low, high = side * planes // 2, (side + 1) * planes // 2
+            at = rows.at[low:high, rows_at(slot, core), :]
+            return rcopy(at, at, rdiag_send.at[side], rdiag_recv.at[side], to_sp, core)
+
+        def row_relay(side):
+            return row_part(sides[side], side, z * plane + sides[1 - side])
 
         def row_core_copy(slot):
             return row_copy(slot, rsend_core.at[slot], here, other)
@@ -617,10 +648,40 @@
             )
 
         row_core_copy(n).start()
-        for step in range(1, plane):
-            offset_copy(step).start()
-
-        wq_copy.wait()
+
+        positions = plane * length
+        at_edge = rows.at[:, positions : positions + edge, :]
+        closing = (n == plane - 1) & (core == cores - 1)
+
+        def edge_up_copy():
+            return rcopy(
+                rows.at[:, positions - edge : positions, :], at_edge, e_send.at[0], e_recv,
+                here + plane, core,
+            )
+
+        def edge_plane_copy(step):
+            return rcopy(at_edge, at_edge, e_send.at[step], e_recv, peer(step), core)
+
+        def edge_core_copy():
+            return rcopy(at_edge, at_edge, e_send.at[plane], e_recv, here, other)
+
+        def edge_arrived():
+            rcopy(at_edge, at_edge, e_send.at[0], e_recv, here, core).wait_recv()
+
+        @pl.when(closing & (z + 1 < planes))
+        def _():
+            edge_up_copy().start()
+
+        for load in loads[10:]:
+            load.wait()
+        for m in range(plane):
+            osend[m, :own_heads] = doff[m * own_heads : (m + 1) * own_heads]
+        obuf[n] = osend[n]
+
+        @pl.when(z == 0)
+        def _():
+            rows[:, plane * length :, :] = jnp.zeros((planes, edge, kblock), bf16)
+
         row_arrived(n, other)
         own_rows = pl.ds(pl.multiple_of(n * length, length), length)
         query = mm(rows[0, own_rows, :], wq[:kblock, :])
@@ -651,10 +712,20 @@
                 for step in range(1, plane):
                     key_plane_copy(d, step).start()
                 key_core_copy(here - d * plane).start()
+
+        @pl.when(closing & (z > 0))
+        def _():
+            edge_arrived()
+            for step in range(1, plane):
+                edge_plane_copy(step).start()
+            edge_core_copy().start()
+
         for step in range(1, plane):
             w_plane_copy(1, step).start()
+        for side in (0, 1):
+            row_plane_copy(side).start()
         for step in range(1, plane):
-            row_plane_copy(step).start()
+            offset_copy(step).start()
 
         def pass_keys(d):
             for step in range(1, plane):
@@ -672,9 +743,17 @@
 
         def visit(first_block, limit):
             count = group_step * cores
-            block = keys[pl.ds(first_block * cores, count)].reshape(size, key_width)
-            lat = block[:, :latent_width]
-            turned = block[:, latent_width : latent_width + ROPE]
+            block = keys[pl.ds(first_block * cores, count)]
+            lat = jnp.concatenate(
+                [
+                    block[:, low * part // 128 : (low + 128) * part // 128].reshape(size, 128)
+                    for low in range(0, latent_width, 128)
+                ],
+                axis=1,
+            )
+            turned = block[:, latent_width * part // 128 :]
+            turned = jnp.concatenate([turned[:, :, :ROPE], turned[:, :, ROPE:]], axis=1)
+            turned = turned.reshape(size, ROPE)
             plain = mm(lat, ku[...]).astype(bf16)
             all_values = mm(lat, vu[...]).astype(bf16)
             if limit is not None:
@@ -700,6 +779,12 @@
                 top[h] = jnp.broadcast_to(new, top.shape[1:])
 
         pass_keys(0)
+
+        @pl.when(z >= 1)
+        def _():
+            pass_keys(1)
+
+        far_weights(0, 1, True)
         other_keys(0)
 
         def near(j, carry):
@@ -709,7 +794,9 @@
         lax.fori_loop(0, n // group_step + 1, near, 0)
 
         def further(d, carry):
-            far_weights(0, d, True)
+            @pl.when(z > d)
+            def _():
+                pass_keys(d + 1)
 
             @pl.when(d == 1)
             def _():
@@ -717,7 +804,6 @@
 
             @pl.when(z >= d)
             def _():
-                pass_keys(d)
                 other_keys(d)
 
                 def inner(j, carry):
@@ -734,72 +820,108 @@
                 summed[h] / total[h][:, :1]
             ).astype(bf16)
 
-        for step in range(1, plane):
-            slot = (n + step) % plane
-            row_arrived(slot, core)
-            row_core_copy(slot).start()
+        @pl.when((z > 0) & (core == cores - 1) & (n < plane - 1))
+        def _():
+            edge_arrived()
+            edge_core_copy().start()
+
+        for side in (0, 1):
+            row_arrived(sides[side], core)
+            row_relay(side).start()
+            row_core_copy(sides[side]).start()
+        for d in range(2, planes - 1):
+            far_weights(0, d, True)
+        far_weights(1, 1, True)
+        for side in (0, 1):
+            row_part(across, side, here).wait_recv()
+        row_core_copy(across).start()
         for step in range(1, plane):
             row_arrived((n + step) % plane, other)
-        tail_at = plane * length - edge
-
-        def edge_copy():
-            return rcopy(
-                rows.at[:, tail_at : tail_at + edge, :], edges, e_send, e_recv,
-                here + plane, core,
-            )
-
-        @pl.when(z + 1 < planes)
+        for d in range(1, planes - 1):
+            far_weights(0, d, False)
+
+        def tile(k):
+            return pl.ds(pl.multiple_of(k * length, length), length)
+
+        def project(p, values, group):
+            low, high = bounds[group]
+            block = wbuf[pl.ds(p * plane, plane), :, low:high]
+            return mm(values, block.reshape(kblock, high - low))
+
+        def sum_near(group, at, store):
+            @pl.when(at_end)
+            def _():
+                out = project(nearest, rows[nearest, at, :], group)
+                for p in range(1, planes - 1):
+                    out += project(nearest + p, rows[nearest + p, at, :], group)
+                store(out, False)
+
+            @pl.when(jnp.logical_not(at_end))
+            def _():
+                out = project(0, rows[0, at, :], group)
+                for p in range(1, planes):
+                    out += project(p, rows[p, at, :], group)
+                store(out, False)
+
+        def sum_far(group, at, store):
+            store(project(farthest, rows[farthest, at, :], group), True)
+
+        strip = (positions + edge) // 5
+        strips = (positions + edge) // strip
+
+        def put(low, count, out, add):
+            at = pl.ds(low, count)
+            projf[at, :] = projf[at, :] + out if add else out
+
+        def every_strip(method):
+            def body(i, carry):
+                def store(out, add):
+                    put(pl.multiple_of(i * strip + edge, edge), strip, out, add)
+
+                method(0, pl.ds(pl.multiple_of(i * strip, edge), strip), store)
+                return carry
+
+            lax.fori_loop(0, strips - 1, body, 0)
+
+        def last_strip(method):
+            low = (strips - 1) * strip
+
+            def store(out, add):
+                put(low + edge, strip - edge, out[: strip - edge], add)
+                put(0, edge, out[strip - edge :], add)
+
+            method(0, slice(low, low + strip), store)
+
+        every_strip(sum_near)
+
+        @pl.when((z > 0) & (core < cores - 1))
         def _():
-            edge_copy().start()
-
-        lane = lax.broadcasted_iota(jnp.int32, (w_step.shape[1], 128), 1)
-        which = lax.broadcasted_iota(jnp.int32, (w_step.shape[1], 128), 0)
+            edge_arrived()
+
+        last_strip(sum_near)
+        lane = lax.broadcasted_iota(jnp.int32, (128, w_step.shape[0]), 0)
+        which = lax.broadcasted_iota(jnp.int32, (128, w_step.shape[0]), 1)
         first_head = (core * plane + n) * own_heads
         chosen = ((which == lane + first_head) & (lane < own_heads)).astype(bf16)
-        stepw[...] = mm(w_step[...], chosen).astype(bf16)
-
-        def tile(k):
-            return pl.ds(pl.multiple_of(k * length, length), length)
+        stepw[...] = mm(chosen, w_step[...]).astype(bf16)
 
         def step_tile(k, carry):
-            raw = mm(rows[0, tile(k), :], stepw[:kblock, :])
-            for p in range(1, planes):
-                raw += mm(rows[p, tile(k), :], stepw[p * kblock : (p + 1) * kblock, :])
+            raw = jnp.zeros((length, 128), f32)
+            for p in range(planes):
+                raw += lax.dot_general(
+                    rows[p, tile(k), :], stepw[:, p * kblock : (p + 1) * kblock],
+                    last_contract, preferred_element_type=f32,
+                )
             steps[k] = jnp.maximum(raw, 0.0) + jnp.log1p(jnp.exp(-jnp.abs(raw)))
             return carry
 
         lax.fori_loop(0, plane, step_tile, 0)
-        for d in range(1, planes):
-            far_weights(1, d, True)
-        for d in range(1, planes):
-            far_weights(0, d, False)
-
-        def project(p, values, group):
-            low, high = bounds[group]
-            block = wbuf[p * plane : (p + 1) * plane, :, low:high]
-            return mm(values, block.reshape(kblock, high - low))
-
-        @pl.when(z > 0)
+        far_weights(0, planes - 1, False)
+
+        @pl.when(at_end)
         def _():
-            rcopy(edges, edges, e_send, e_recv, here, core).wait_recv()
-            first = project(0, edges[0], 0)
-            for p in range(1, planes):
-                first += project(p, edges[p], 0)
-            projf[:edge, :] = first.astype(bf16).astype(f32)
-
-        @pl.when(z == 0)
-        def _():
-            projf[:edge, :] = jnp.zeros((edge, lower), f32)
-
-        def project_tile(k, carry):
-            out = project(0, rows[0, tile(k), :], 0)
-            for p in range(1, planes):
-                out += project(p, rows[p, tile(k), :], 0)
-            at = pl.ds(pl.multiple_of(k * length + edge, edge), length)
-            projf[at, :] = out.astype(bf16).astype(f32)
-            return carry
-
-        lax.fori_loop(0, plane, project_tile, 0)
+            every_strip(sum_far)
+            last_strip(sum_far)
 
         taps = jnp.concatenate(
             [
@@ -814,7 +936,7 @@
             base = pl.ds(pl.multiple_of(k * length, length), length + edge)
             for low in range(0, lower, 128):
                 at = slice(low, low + 128)
-                values = projf[base, at]
+                values = projf[base, at].astype(bf16).astype(f32)
                 result = jnp.zeros((length, 128), f32)
                 for i in range(span):
                     shift = edge - span + 1 + i
@@ -911,8 +1033,20 @@
                 for copy in state_copies(d):
                     copy.start()
 
-        for d in range(1, planes):
+        for d in range(2, planes):
+            far_weights(1, d, True)
+        for d in range(1, planes - 1):
             far_weights(1, d, False)
+
+        def gate_tile(k, carry):
+            def store(out, add):
+                gatef[tile(k), :] = out
+
+            sum_near(1, tile(k), store)
+            return carry
+
+        lax.fori_loop(0, plane, gate_tile, 0)
+        far_weights(1, planes - 1, False)
         incoming[...] = jnp.zeros(incoming.shape, f32)
         for p in range(planes - 1):
             @pl.when(p < z)
@@ -937,11 +1071,17 @@
             )
 
         def finish(i, carry):
-            k = (n + 1 + i) % plane
-            gate = project(0, rows[0, tile(k), :], 1)
-            for p in range(1, planes):
-                gate += project(p, rows[p, tile(k), :], 1)
-            gate = gate.astype(bf16).astype(f32)
+            flip = plane - 1 - i
+            k = (n // 2 + flip // 2) % 2 * 2 + (n + flip) % 2
+
+            @pl.when(at_end)
+            def _():
+                def store(out, add):
+                    gatef[tile(k), :] = gatef[tile(k), :] + out
+
+                sum_far(1, tile(k), store)
+
+            gate = gatef[tile(k), :].astype(bf16).astype(f32)
             entered = (
                 before[k] + per_row(jnp.exp(decayed[k][:1])) * incoming[...]
             ).astype(bf16)
@@ -986,15 +1126,26 @@
         for step in range(1, plane):
             for group in (0, 1):
                 w_plane_copy(group, step).wait_send()
-            row_plane_copy(step).wait_send()
             offset_copy(step).wait_send()
             out_copy((n + step) % plane).wait_send()
+        for side in (0, 1):
+            row_plane_copy(side).wait_send()
+            row_relay(side).wait_send()
         for slot in range(plane):
             row_core_copy(slot).wait_send()
 
-        @pl.when(z + 1 < planes)
+        @pl.when(closing & (z + 1 < planes))
         def _():
-            edge_copy().wait_send()
+            edge_up_copy().wait_send()
+
+        @pl.when(closing & (z > 0))
+        def _():
+            for step in range(1, plane):
+                edge_plane_copy(step).wait_send()
+
+        @pl.when((z > 0) & (core == cores - 1))
+        def _():
+            edge_core_copy().wait_send()
 
         for up in (0, 1):
             for p in range(planes):
@@ -1007,33 +1158,57 @@
     vmem = pl.BlockSpec(memory_space=pltpu.VMEM)
     smem = pl.BlockSpec(memory_space=pltpu.SMEM)
     hbm = pl.BlockSpec(memory_space=pltpu.HBM)
-    freqs = theta ** (-jnp.arange(half, dtype=f32) * 2.0 / ROPE)
+    freqs = np.float32(theta) ** (-np.arange(half, dtype=np.float32) * np.float32(2.0 / ROPE))
+    inputs = (
+        scan_input,
+        scan_write,
+        scan_read,
+        scan_gate,
+        tokens,
+        mix_gain[None, :],
+        compressed_projection,
+        compressed_norm_gain[None, :],
+        rope_proj.T,
+        jnp.asarray(freqs[None, :], f32),
+        query_proj,
+        key_up,
+        value_up_weight,
+        decay_offset.T,
+        step_proj.T,
+        conv_input,
+        conv_write,
+        conv_read,
+        group_gain[None, :],
+    )
+    loaded = len(inputs)
     dma = pltpu.SemaphoreType.DMA
     positions = plane * length
-    return pl.pallas_call(
+    results = (
+        jax.ShapeDtypeStruct((length, heads * VALUE_WIDTH), bf16),
+        jax.ShapeDtypeStruct((length, scan_input.shape[1]), bf16),
+    )
+    outs = pl.pallas_call(
         kernel,
-        out_shape=(
-            jax.ShapeDtypeStruct((length, heads * VALUE_WIDTH), bf16),
-            jax.ShapeDtypeStruct((length, scan_input.shape[1]), bf16),
-        ),
-        in_specs=[vmem, vmem, hbm] + [vmem] * 13 + [smem, vmem, smem, vmem, vmem],
+        out_shape=results,
+        in_specs=[hbm] * loaded + [smem, smem],
         out_specs=(vmem, vmem),
-        scratch_shapes=[
-            pltpu.VMEM(query_proj.shape, bf16),
+        scratch_shapes=[pltpu.VMEM(value.shape, value.dtype) for value in inputs]
+        + [
+            dma((loaded,)),
             pltpu.VMEM((plane, depth, wide), bf16),
             pltpu.VMEM((devices, depth, wide), bf16),
-            pltpu.VMEM((planes, positions, kblock), bf16),
-            pltpu.VMEM((planes, edge, kblock), bf16),
-            pltpu.VMEM((devices * cores, part, key_width), bf16),
+            pltpu.VMEM((planes, positions + edge, kblock), bf16),
+            pltpu.VMEM((devices * cores, key_rows, 128), bf16),
             pltpu.VMEM((heads, length, whole), bf16),
             pltpu.VMEM((heads, length, 128), f32),
             pltpu.VMEM((heads, length, 128), f32),
             pltpu.VMEM((heads, length, VALUE_WIDTH), f32),
-            pltpu.VMEM((width, 128), bf16),
+            pltpu.VMEM((128, width), bf16),
             pltpu.VMEM((plane, length, 128), f32),
             pltpu.VMEM((plane, 8, length), f32),
             pltpu.VMEM((plane, 8, length), f32),
             pltpu.VMEM((edge + positions, lower), f32),
+            pltpu.VMEM((positions, hw), f32),
             pltpu.VMEM((positions, lower), bf16),
             pltpu.VMEM((positions, hw), f32),
             pltpu.VMEM((plane, length, 128), f32),
@@ -1047,20 +1222,21 @@
             pltpu.VMEM((planes, 8, 128), f32),
             pltpu.VMEM((own_heads * SSM_DIM, SSM_STATE), f32),
             pltpu.VMEM((plane, length, hw), bf16),
-            dma,
             dma((2, plane)),
             dma((2, devices)),
             dma((2, 2, devices)),
             dma((planes,)),
-            dma((planes * plane,)),
+            dma((devices,)),
             dma((devices,)),
             dma((devices * cores,)),
+            dma((2,)),
+            dma((plane,)),
+            dma((plane * cores,)),
+            dma((2,)),
+            dma((2,)),
             dma((plane,)),
             dma((plane,)),
-            dma((plane * cores,)),
-            dma((plane,)),
-            dma((plane,)),
-            dma,
+            dma((plane + 1,)),
             dma,
             dma((planes,)),
             dma((planes,)),
@@ -1073,29 +1249,40 @@
             collective_id=1, has_side_effects=True, vmem_limit_bytes=60 * 1024 * 1024
         ),
         name="fused",
-    )(
-        tokens,
-        mix_gain[None, :],
-        query_proj,
-        compressed_projection,
-        compressed_norm_gain[None, :],
-        rope_proj,
-        key_up,
-        value_up_weight,
-        scan_input,
-        scan_gate,
-        scan_write,
-        scan_read,
-        step_proj,
-        conv_input,
-        conv_write,
-        conv_read,
-        decay_log,
-        decay_offset,
-        skip_gain,
-        group_gain[None, :],
-        freqs[None, :],
-    )
+    )(*inputs, decay_log, skip_gain)
+
+    def settle(a_in, b_in, a_out, b_out, a_mid, b_mid, ins, leaves):
+        rows_each = length // 2
+        pieces = [(a_in, a_mid, a_out)] + [
+            tuple(ref.at[low : low + rows_each] for ref in (b_in, b_mid, b_out))
+            for low in (0, rows_each)
+        ]
+        first = [
+            pltpu.make_async_copy(source, middle, ins.at[i])
+            for i, (source, middle, _) in enumerate(pieces)
+        ]
+        second = [
+            pltpu.make_async_copy(middle, target, leaves.at[i])
+            for i, (_, middle, target) in enumerate(pieces)
+        ]
+        for copy in first:
+            copy.start()
+        for copy, after in zip(first, second):
+            copy.wait()
+            after.start()
+        for copy in second:
+            copy.wait()
+
+    return pl.pallas_call(
+        settle,
+        out_shape=results,
+        in_specs=[hbm, hbm],
+        out_specs=(hbm, hbm),
+        scratch_shapes=[pltpu.VMEM(value.shape, value.dtype) for value in results]
+        + [dma((3,)), dma((3,))],
+        compiler_params=pltpu.CompilerParams(vmem_limit_bytes=60 * 1024 * 1024),
+        name="settle",
+    )(*outs)
 
 
 def shards(
@@ -1128,7 +1315,7 @@
     across, within = sp_index // plane, sp_index % plane
     own_groups = groups // plane
     direct = plane > 1
-    if direct and cores == 2 and own_groups == 1 and plane % 2 == 0 and planes > 1:
+    if direct and cores == 2 and own_groups == 1 and plane == 4 and planes > 1:
         return fused(
             plane,
             tokens,

time: 100 us -> 84 us (0.84)
  local copies, waits for them, and re-layouts: 8.86 us -> 0 us
  Pallas kernels: 88.9 us -> 82.1 us
    unnamed x5 -> x0, local copies, waits for them, and re-layouts: 8.86 us -> none
    pallas_call x1 -> x2, Pallas kernels: 88.9 us -> 82.1 us  [the longest x1 80.2 us: fused(): pl.pallas_call(kernel, out_shape=results, in_specs=[hbm] * loaded + [smem...]
where the time goes in v2:
time: 84 us; the launch traced here: 82.8 us
  Pallas kernels  82.1 us (98%)
    pallas_call x1, Pallas kernels, fused(): pl.pallas_call(kernel, out_shape=results, in_specs=[hbm] * loaded + [smem...  80.2 us
    pallas_call x1, Pallas kernels, fused(): pl.pallas_call(settle, out_shape=results, in_specs=[hbm, hbm], out_specs=...  1.88 us

profile of v2, /device:TPU:28, one launch (start us, length us, event | category | flops | bytes accessed | tf_op | source)
XLA Modules:
  0.0 82.8 jit_solution(5884911435646101974)
XLA Ops:
  0.6 80.2 %fused.1 = (bf16[256,512]{1,0:T(8,128)(2,1)}, bf16[256,1024]{1,0:T(8,128)(2,1)}) custom-call(bf16[128,1024]{1,0:T(8,128)(2,1)} %refs_0_.1, bf16[128,512]{1,0:T(8,128)(2,1)} %refs_1_.1, bf16[128,512]{1,0:T(8,128)(2,1)} %refs_2_.1, bf16[128,1024]{1,0:T(8,128)(2,1)} %refs_3_.1, bf16[128,2048]{1,0:T(8,128)(2,1)} %refs_4_.1, f32[1,2048]{1,0:T(1,128)} %bitcast.9, ...), custom_call_target="tpu_custom_call" | custom-call | tf_op jit(solution)/shard_map/fused/pallas_call | solution.py:1190
  80.9 1.9 %settle.1 = (bf16[256,512]{1,0:T(8,128)(2,1)}, bf16[256,1024]{1,0:T(8,128)(2,1)}) custom-call(bf16[256,512]{1,0:T(8,128)(2,1)} %get-tuple-element.4.a_in, bf16[256,1024]{1,0:T(8,128)(2,1)} %get-tuple-element.5.b_in), custom_call_target="tpu_custom_call" | custom-call | tf_op jit(solution)/shard_map/settle/pallas_call | solution.py:1276

commit v3 on v2

--- a/solution.py
+++ b/solution.py
@@ -428,21 +428,20 @@
     def kernel(
         *refs
     ):
-        sources, (dlog, skip) = refs[:loaded], refs[loaded : loaded + 2]
-        att_out, scan_out = refs[loaded + 2 : loaded + 4]
-        targets = refs[loaded + 4 : 2 * loaded + 4]
+        sources, (att_out, scan_out) = refs[:loaded], refs[loaded : loaded + 2]
+        targets = refs[loaded + 2 : 2 * loaded + 2]
         (
             w_in, w_write, w_read, w_gate, tok, mix, comp, comp_gain, rope, freqs, wq, ku, vu,
-            doff, w_step, t_in, t_write, t_read, ggain,
+            doff, w_step, t_in, t_write, t_read, ggain, dlog, skip,
         ) = targets
         (
             load_sem, packed, wbuf, rows, keys, q_all, top, total, summed, stepw, steps, osend,
             obuf, projf, gatef, cbuf, ybuf, runs, before, decayed, state, dsum, ssend, tsend,
             srecv, trecv, incoming, stage, wsend, wrecv, zsend, ksend_up, ksend_plane,
             ksend_core, krecv, rsend, rsend_core, rrecv, rdiag_send,
-            rdiag_recv, o_send, o_recv, e_send, e_recv, s_send, s_recv, t_send, t_recv,
+            rhalf, o_send, o_recv, e_send, e_recv, s_send, s_recv, t_send, t_recv,
             out_send, out_recv,
-        ) = refs[2 * loaded + 4 :]
+        ) = refs[2 * loaded + 2 :]
         here, core = lax.axis_index("sp"), lax.axis_index("tp")
         z, n = here // plane, here % plane
         other = cores - 1 - core
@@ -555,7 +554,7 @@
                     def _():
                         z_copy(group, index, up).start()
 
-        def far_weights(group, d, forward):
+        def far_weights(group, d, forward, pieces=range(plane)):
             for up in (0, 1):
                 source = z - d if up else z + d
                 exists = (source >= 0) & (source < planes)
@@ -563,8 +562,8 @@
 
                 @pl.when(exists & gate)
                 def _():
-                    for q in range(plane):
-                        index = source * plane + q
+                    for step in pieces:
+                        index = source * plane + (n - step + plane) % plane
                         w_arrived(group, index)
                         if forward:
                             z_copy(group, index, up).start()
@@ -572,6 +571,7 @@
         for step in range(1, plane):
             w_plane_copy(0, step).start()
         own_weights(0, (0,))
+        own_weights(1, (0,))
 
         for load in loads[4:10]:
             load.wait()
@@ -614,24 +614,34 @@
             @pl.when(z + d < planes)
             def _():
                 key_up_copy(d).start()
-        for step in range(1, plane):
-            key_plane_copy(0, step).start()
         key_core_copy(here).start()
 
         def row_copy(slot, ss, to_sp, to_c):
             at = rows.at[:, rows_at(slot, core), :]
             return rcopy(at, at, ss, rrecv.at[slot * cores + core], to_sp, to_c)
 
-        def row_plane_copy(side):
-            return row_copy(n, rsend.at[side], z * plane + sides[side], core)
-
-        def row_part(slot, side, to_sp):
-            low, high = side * planes // 2, (side + 1) * planes // 2
+        def row_part(slot, part_of, ss, rs, to_sp):
+            low, high = part_of * planes // 2, (part_of + 1) * planes // 2
             at = rows.at[low:high, rows_at(slot, core), :]
-            return rcopy(at, at, rdiag_send.at[side], rdiag_recv.at[side], to_sp, core)
+            return rcopy(at, at, ss, rs, to_sp, core)
+
+        def row_plane_copy(side, part_of):
+            return row_part(
+                n, part_of, rsend.at[side, part_of], rhalf.at[n, part_of],
+                z * plane + sides[side],
+            )
+
+        def row_half_arrived(slot, part_of):
+            row_part(
+                slot, part_of, rsend.at[0, 0], rhalf.at[slot, part_of], here
+            ).wait_recv()
 
         def row_relay(side):
-            return row_part(sides[side], side, z * plane + sides[1 - side])
+            slot = sides[side]
+            return row_part(
+                slot, side, rdiag_send.at[side], rhalf.at[slot, side],
+                z * plane + sides[1 - side],
+            )
 
         def row_core_copy(slot):
             return row_copy(slot, rsend_core.at[slot], here, other)
@@ -705,6 +715,8 @@
         summed[...] = jnp.zeros(summed.shape, f32)
 
         own_weights(0, range(1, plane))
+        for step in range(1, plane):
+            key_plane_copy(0, step).start()
         for d in range(1, planes):
             @pl.when(z >= d)
             def _():
@@ -722,8 +734,9 @@
 
         for step in range(1, plane):
             w_plane_copy(1, step).start()
-        for side in (0, 1):
-            row_plane_copy(side).start()
+        for first in (0, 1):
+            for side in (0, 1):
+                row_plane_copy(side, (side + first) % 2).start()
         for step in range(1, plane):
             offset_copy(step).start()
 
@@ -793,14 +806,16 @@
 
         lax.fori_loop(0, n // group_step + 1, near, 0)
 
+        late = min(2, planes - 1)
+
         def further(d, carry):
             @pl.when(z > d)
             def _():
                 pass_keys(d + 1)
 
-            @pl.when(d == 1)
+            @pl.when(d == late)
             def _():
-                own_weights(1, range(plane))
+                own_weights(1, range(1, plane))
 
             @pl.when(z >= d)
             def _():
@@ -826,17 +841,14 @@
             edge_core_copy().start()
 
         for side in (0, 1):
-            row_arrived(sides[side], core)
+            row_half_arrived(sides[side], side)
             row_relay(side).start()
+        for side in (0, 1):
+            row_half_arrived(sides[side], 1 - side)
             row_core_copy(sides[side]).start()
         for d in range(2, planes - 1):
             far_weights(0, d, True)
         far_weights(1, 1, True)
-        for side in (0, 1):
-            row_part(across, side, here).wait_recv()
-        row_core_copy(across).start()
-        for step in range(1, plane):
-            row_arrived((n + step) % plane, other)
         for d in range(1, planes - 1):
             far_weights(0, d, False)
 
@@ -866,46 +878,26 @@
         def sum_far(group, at, store):
             store(project(farthest, rows[farthest, at, :], group), True)
 
-        strip = (positions + edge) // 5
-        strips = (positions + edge) // strip
-
-        def put(low, count, out, add):
-            at = pl.ds(low, count)
-            projf[at, :] = projf[at, :] + out if add else out
-
-        def every_strip(method):
-            def body(i, carry):
-                def store(out, add):
-                    put(pl.multiple_of(i * strip + edge, edge), strip, out, add)
-
-                method(0, pl.ds(pl.multiple_of(i * strip, edge), strip), store)
-                return carry
-
-            lax.fori_loop(0, strips - 1, body, 0)
-
-        def last_strip(method):
-            low = (strips - 1) * strip
-
+        def into(low, count):
             def store(out, add):
-                put(low + edge, strip - edge, out[: strip - edge], add)
-                put(0, edge, out[strip - edge :], add)
-
-            method(0, slice(low, low + strip), store)
-
-        every_strip(sum_near)
-
-        @pl.when((z > 0) & (core < cores - 1))
-        def _():
-            edge_arrived()
-
-        last_strip(sum_near)
+                at = pl.ds(low, count)
+                projf[at, :] = projf[at, :] + out if add else out
+
+            return store
+
+        def edge_sum(method):
+            method(0, pl.ds(positions, edge), into(0, edge))
+
+        def tile_sum(method, k):
+            method(0, tile(k), into(pl.multiple_of(k * length + edge, edge), length))
+
         lane = lax.broadcasted_iota(jnp.int32, (128, w_step.shape[0]), 0)
         which = lax.broadcasted_iota(jnp.int32, (128, w_step.shape[0]), 1)
         first_head = (core * plane + n) * own_heads
         chosen = ((which == lane + first_head) & (lane < own_heads)).astype(bf16)
         stepw[...] = mm(chosen, w_step[...]).astype(bf16)
 
-        def step_tile(k, carry):
+        def step_tile(k):
             raw = jnp.zeros((length, 128), f32)
             for p in range(planes):
                 raw += lax.dot_general(
@@ -913,15 +905,48 @@
                     last_contract, preferred_element_type=f32,
                 )
             steps[k] = jnp.maximum(raw, 0.0) + jnp.log1p(jnp.exp(-jnp.abs(raw)))
+
+        @pl.when((z > 0) & (core < cores - 1))
+        def _():
+            edge_arrived()
+
+        edge_sum(sum_near)
+
+        def turned_slot(flip):
+            return (n // 2 + flip // 2) % 2 * 2 + (n + flip) % 2
+
+        def first_sums(flip, carry):
+            slot = turned_slot(flip)
+
+            @pl.when(flip == plane - 1)
+            def _():
+                for part_of in (0, 1):
+                    row_half_arrived(across, part_of)
+                row_core_copy(across).start()
+
+            @pl.when(flip > 0)
+            def _():
+                row_arrived(slot, other)
+
+            tile_sum(sum_near, slot)
+            step_tile(slot)
             return carry
 
-        lax.fori_loop(0, plane, step_tile, 0)
+        lax.fori_loop(0, plane, first_sums, 0)
         far_weights(0, planes - 1, False)
 
         @pl.when(at_end)
         def _():
-            every_strip(sum_far)
-            last_strip(sum_far)
+            edge_sum(sum_far)
+
+            def last_sums(k, carry):
+                tile_sum(sum_far, k)
+                return carry
+
+            lax.fori_loop(0, plane, last_sums, 0)
+
+        for d in range(2, planes - 1):
+            far_weights(1, d, True, range(plane - 1))
 
         taps = jnp.concatenate(
             [
@@ -1017,8 +1042,9 @@
 
         lax.fori_loop(0, plane, scan_tile, 0)
 
-        ssend[...] = state[...].astype(bf16)
-        tsend[...] = dsum[...]
+        def state_arrived(p):
+            rcopy(ssend, srecv.at[p], s_send.at[0], s_recv.at[p], here, core).wait_recv()
+            rcopy(tsend, trecv.at[p], t_send.at[0], t_recv.at[p], here, core).wait_recv()
 
         def state_copies(d):
             to = here + d * plane
@@ -1027,14 +1053,30 @@
                 rcopy(tsend, trecv.at[z], t_send.at[d], t_recv.at[z], to, core),
             )
 
+        def to_send(d):
+            return (z + d < planes) & ((z == 0) | (d == 1))
+
+        @pl.when((z > 1) & (z + 1 < planes))
+        def _():
+            state_arrived(z - 1)
+            ssend[...] = (
+                per_row(jnp.exp(dsum[:1])) * srecv[z - 1].astype(f32) + state[...]
+            ).astype(bf16)
+            tsend[...] = dsum[...] + trecv[z - 1]
+
+        @pl.when(z <= 1)
+        def _():
+            ssend[...] = state[...].astype(bf16)
+            tsend[...] = dsum[...]
+
         for d in range(1, planes):
-            @pl.when(z + d < planes)
+            @pl.when(to_send(d))
             def _():
                 for copy in state_copies(d):
                     copy.start()
 
-        for d in range(2, planes):
-            far_weights(1, d, True)
+        for d in range(2, planes - 1):
+            far_weights(1, d, True, range(plane - 1, plane))
         for d in range(1, planes - 1):
             far_weights(1, d, False)
 
@@ -1046,42 +1088,26 @@
             return carry
 
         lax.fori_loop(0, plane, gate_tile, 0)
-        far_weights(1, planes - 1, False)
-        incoming[...] = jnp.zeros(incoming.shape, f32)
-        for p in range(planes - 1):
-            @pl.when(p < z)
-            def _():
-                rcopy(
-                    ssend, srecv.at[p], s_send.at[0], s_recv.at[p], here, core
-                ).wait_recv()
-                rcopy(
-                    tsend, trecv.at[p], t_send.at[0], t_recv.at[p], here, core
-                ).wait_recv()
-                incoming[...] = per_row(jnp.exp(trecv[p][:1])) * incoming[...] + srecv[
-                    p
-                ].astype(f32)
-
-        own_columns = pl.ds(pl.multiple_of(n * hw, hw), hw)
-        gain = ggain[:, own_columns]
-
-        def out_copy(k):
-            return rcopy(
-                stage.at[k], scan_out.at[:, own_columns], out_send.at[k], out_recv.at[n],
-                z * plane + k, core,
-            )
-
-        def finish(i, carry):
-            flip = plane - 1 - i
-            k = (n // 2 + flip // 2) % 2 * 2 + (n + flip) % 2
-
-            @pl.when(at_end)
-            def _():
-                def store(out, add):
-                    gatef[tile(k), :] = gatef[tile(k), :] + out
-
-                sum_far(1, tile(k), store)
-
-            gate = gatef[tile(k), :].astype(bf16).astype(f32)
+        @pl.when((z > 1) & (z + 1 == planes))
+        def _():
+            state_arrived(z - 1)
+
+        @pl.when(z > 0)
+        def _():
+            state_arrived(0)
+
+        @pl.when(z == 1)
+        def _():
+            incoming[...] = srecv[0].astype(f32)
+
+        @pl.when(z > 1)
+        def _():
+            incoming[...] = (
+                per_row(jnp.exp(trecv[z - 1][:1])) * srecv[0].astype(f32)
+                + srecv[z - 1].astype(f32)
+            )
+
+        def carry_tile(k, carry):
             entered = (
                 before[k] + per_row(jnp.exp(decayed[k][:1])) * incoming[...]
             ).astype(bf16)
@@ -1089,7 +1115,36 @@
                 cbuf[tile(k), hw + ww : lower], entered, last_contract,
                 preferred_element_type=f32,
             )
-            mixed = ybuf[tile(k), :] + carried * per_lane(jnp.exp(runs[k]))
+            ybuf[tile(k), :] = ybuf[tile(k), :] + carried * per_lane(jnp.exp(runs[k]))
+            return carry
+
+        @pl.when(z == 0)
+        def _():
+            incoming[...] = jnp.zeros(incoming.shape, f32)
+
+        lax.fori_loop(0, plane, carry_tile, 0)
+        far_weights(1, planes - 1, False)
+        own_columns = pl.ds(pl.multiple_of(n * hw, hw), hw)
+        gain = ggain[:, own_columns]
+
+        def out_copy(k):
+            return rcopy(
+                stage.at[k], scan_out.at[:, own_columns], out_send.at[k], out_recv.at[n],
+                z * plane + k, core,
+            )
+
+        def finish(i, carry):
+            k = turned_slot(plane - 1 - i)
+
+            @pl.when(at_end)
+            def _():
+                def store(out, add):
+                    gatef[tile(k), :] = gatef[tile(k), :] + out
+
+                sum_far(1, tile(k), store)
+
+            gate = gatef[tile(k), :].astype(bf16).astype(f32)
+            mixed = ybuf[tile(k), :]
             gated = mixed * (gate * jax.nn.sigmoid(gate))
             out = normed_rows(gated, gain, hw).astype(bf16)
             stage[k] = out
@@ -1114,8 +1169,12 @@
             @pl.when(z + d < planes)
             def _():
                 key_up_copy(d).wait_send()
+
+            @pl.when(to_send(d))
+            def _():
                 for copy in state_copies(d):
                     copy.wait_send()
+
         for d in range(planes):
             @pl.when(z >= d)
             def _():
@@ -1129,7 +1188,8 @@
             offset_copy(step).wait_send()
             out_copy((n + step) % plane).wait_send()
         for side in (0, 1):
-            row_plane_copy(side).wait_send()
+            for part_of in (0, 1):
+                row_plane_copy(side, part_of).wait_send()
             row_relay(side).wait_send()
         for slot in range(plane):
             row_core_copy(slot).wait_send()
@@ -1156,7 +1216,6 @@
                             z_copy(group, p * plane + q, up).wait_send()
 
     vmem = pl.BlockSpec(memory_space=pltpu.VMEM)
-    smem = pl.BlockSpec(memory_space=pltpu.SMEM)
     hbm = pl.BlockSpec(memory_space=pltpu.HBM)
     freqs = np.float32(theta) ** (-np.arange(half, dtype=np.float32) * np.float32(2.0 / ROPE))
     inputs = (
@@ -1179,6 +1238,8 @@
         conv_write,
         conv_read,
         group_gain[None, :],
+        decay_log,
+        skip_gain,
     )
     loaded = len(inputs)
     dma = pltpu.SemaphoreType.DMA
@@ -1190,9 +1251,10 @@
     outs = pl.pallas_call(
         kernel,
         out_shape=results,
-        in_specs=[hbm] * loaded + [smem, smem],
+        in_specs=[hbm] * loaded,
         out_specs=(vmem, vmem),
-        scratch_shapes=[pltpu.VMEM(value.shape, value.dtype) for value in inputs]
+        scratch_shapes=[pltpu.VMEM(value.shape, value.dtype) for value in inputs[:-2]]
+        + [pltpu.SMEM(value.shape, value.dtype) for value in inputs[-2:]]
         + [
             dma((loaded,)),
             pltpu.VMEM((plane, depth, wide), bf16),
@@ -1229,11 +1291,11 @@
             dma((devices,)),
             dma((devices,)),
             dma((devices * cores,)),
-            dma((2,)),
+            dma((2, 2)),
             dma((plane,)),
             dma((plane * cores,)),
             dma((2,)),
-            dma((2,)),
+            dma((plane, 2)),
             dma((plane,)),
             dma((plane,)),
             dma((plane + 1,)),
@@ -1246,41 +1308,28 @@
             dma((plane,)),
         ],
         compiler_params=pltpu.CompilerParams(
-            collective_id=1, has_side_effects=True, vmem_limit_bytes=60 * 1024 * 1024
+            collective_id=1, has_side_effects=True, vmem_limit_bytes=48 * 1024 * 1024
         ),
         name="fused",
-    )(*inputs, decay_log, skip_gain)
-
-    def settle(a_in, b_in, a_out, b_out, a_mid, b_mid, ins, leaves):
-        rows_each = length // 2
-        pieces = [(a_in, a_mid, a_out)] + [
-            tuple(ref.at[low : low + rows_each] for ref in (b_in, b_mid, b_out))
-            for low in (0, rows_each)
+    )(*[pltpu.with_memory_space_constraint(value, pltpu.HBM) for value in inputs])
+
+    def settle(a_in, b_in, a_out, b_out, sems):
+        copies = [
+            pltpu.make_async_copy(a_in, a_out, sems.at[0]),
+            pltpu.make_async_copy(b_in, b_out, sems.at[1]),
         ]
-        first = [
-            pltpu.make_async_copy(source, middle, ins.at[i])
-            for i, (source, middle, _) in enumerate(pieces)
-        ]
-        second = [
-            pltpu.make_async_copy(middle, target, leaves.at[i])
-            for i, (_, middle, target) in enumerate(pieces)
-        ]
-        for copy in first:
+        for copy in copies:
             copy.start()
-        for copy, after in zip(first, second):
-            copy.wait()
-            after.start()
-        for copy in second:
+        for copy in copies:
             copy.wait()
 
     return pl.pallas_call(
         settle,
         out_shape=results,
-        in_specs=[hbm, hbm],
+        in_specs=[vmem, vmem],
         out_specs=(hbm, hbm),
-        scratch_shapes=[pltpu.VMEM(value.shape, value.dtype) for value in results]
-        + [dma((3,)), dma((3,))],
-        compiler_params=pltpu.CompilerParams(vmem_limit_bytes=60 * 1024 * 1024),
+        scratch_shapes=[dma((2,))],
+        compiler_params=pltpu.CompilerParams(vmem_limit_bytes=4 * 1024 * 1024),
         name="settle",
     )(*outs)
 

time: 84 us -> 75.7 us (0.901); the launches traced: 82.8 us -> 75.5 us
  Pallas kernels: 82.1 us -> 74.9 us
    pallas_call x2, Pallas kernels: 82.1 us -> 74.9 us  [the longest x1 74 us: fused(): pl.pallas_call(kernel, out_shape=results, in_specs=[hbm] * loaded, out_sp...]
where the time goes in v3:
time: 75.7 us; the launch traced here: 75.5 us
  Pallas kernels  74.9 us (99%)
    pallas_call x1, Pallas kernels, fused(): pl.pallas_call(kernel, out_shape=results, in_specs=[hbm] * loaded, out_sp...  74 us

profile of v3, /device:TPU:28, one launch (start us, length us, event | category | flops | bytes accessed | tf_op | source)
XLA Modules:
  0.0 75.5 jit_solution(1597580246765800711)
XLA Ops:
  0.6 74.0 %fused.1 = (bf16[256,512]{1,0:T(8,128)(2,1)S(1)}, bf16[256,1024]{1,0:T(8,128)(2,1)S(1)}) custom-call(bf16[128,1024]{1,0:T(8,128)(2,1)} %refs_0_.1, bf16[128,512]{1,0:T(8,128)(2,1)} %refs_1_.1, bf16[128,512]{1,0:T(8,128)(2,1)} %refs_2_.1, bf16[128,1024]{1,0:T(8,128)(2,1)} %refs_3_.1, bf16[128,2048]{1,0:T(8,128)(2,1)} %refs_4_.1, f32[1,2048]{1,0:T(1,128)} %bitcast.9, ...), custom_call_target="tpu_custom_call" | custom-call | tf_op jit(solution)/shard_map/fused/pallas_call | solution.py:1251
  74.6 0.9 %settle.1 = (bf16[256,512]{1,0:T(8,128)(2,1)}, bf16[256,1024]{1,0:T(8,128)(2,1)}) custom-call(bf16[256,512]{1,0:T(8,128)(2,1)S(1)} %get-tuple-element.4.a_in, bf16[256,1024]{1,0:T(8,128)(2,1)S(1)} %get-tuple-element.5.b_in), custom_call_target="tpu_custom_call" | custom-call | tf_op jit(solution)/shard_map/settle/pallas_call | solution.py:1326

commit v4 on v3

--- a/solution.py
+++ b/solution.py
@@ -414,7 +414,7 @@
     half = ROPE // 2
     scale = whole ** (-0.5)
     span = conv_input.shape[0]
-    edge = 16
+    edge = 8
     bf16, f32 = jnp.bfloat16, jnp.float32
     MESH = pl.DeviceIdType.MESH
     last_contract = (((1,), (1,)), ((), ()))
@@ -463,6 +463,9 @@
                 device_id=(sp, c), device_id_type=MESH,
             )
 
+        def turned_slot(flip):
+            return (n // 2 + flip // 2) % 2 * 2 + (n + flip) % 2
+
         def peer(step):
             return z * plane + (n + step) % plane
 
@@ -529,7 +532,7 @@
 
         def w_plane_copy(group, step):
             low, high = bounds[group]
-            goal = (n + step) % plane
+            goal = turned_slot(step)
             return rcopy(
                 packed.at[goal, :, low:high], chunk(group, here), wsend.at[group, step],
                 wrecv.at[group, here], z * plane + goal, core,
@@ -546,7 +549,7 @@
 
         def own_weights(group, steps_of):
             for step in steps_of:
-                index = z * plane + (n - step + plane) % plane
+                index = z * plane + turned_slot(step)
                 if step:
                     w_arrived(group, index)
                 for up in (0, 1):
@@ -554,8 +557,8 @@
                     def _():
                         z_copy(group, index, up).start()
 
-        def far_weights(group, d, forward, pieces=range(plane)):
-            for up in (0, 1):
+        def far_weights(group, d, forward, pieces=range(plane), ways=(0, 1)):
+            for up in ways:
                 source = z - d if up else z + d
                 exists = (source >= 0) & (source < planes)
                 gate = has_next(up) if forward else jnp.logical_not(has_next(up))
@@ -563,7 +566,7 @@
                 @pl.when(exists & gate)
                 def _():
                     for step in pieces:
-                        index = source * plane + (n - step + plane) % plane
+                        index = source * plane + turned_slot(step)
                         w_arrived(group, index)
                         if forward:
                             z_copy(group, index, up).start()
@@ -815,7 +818,8 @@
 
             @pl.when(d == late)
             def _():
-                own_weights(1, range(1, plane))
+                for far in range(2, planes - 1):
+                    far_weights(0, far, True, range(plane // 2))
 
             @pl.when(z >= d)
             def _():
@@ -826,6 +830,16 @@
                     return carry
 
                 lax.fori_loop(0, plane // group_step, inner, 0)
+
+            @pl.when(d == late)
+            def _():
+                for far in range(2, planes - 1):
+                    far_weights(0, far, True, range(plane // 2, plane))
+                own_weights(1, range(1, plane))
+
+            @pl.when((d == late) & (z == 1))
+            def _():
+                far_weights(1, 1, True, ways=(1,))
 
             return carry
 
@@ -846,9 +860,6 @@
         for side in (0, 1):
             row_half_arrived(sides[side], 1 - side)
             row_core_copy(sides[side]).start()
-        for d in range(2, planes - 1):
-            far_weights(0, d, True)
-        far_weights(1, 1, True)
         for d in range(1, planes - 1):
             far_weights(0, d, False)
 
@@ -912,9 +923,6 @@
 
         edge_sum(sum_near)
 
-        def turned_slot(flip):
-            return (n // 2 + flip // 2) % 2 * 2 + (n + flip) % 2
-
         def first_sums(flip, carry):
             slot = turned_slot(flip)
 
@@ -933,6 +941,12 @@
             return carry
 
         lax.fori_loop(0, plane, first_sums, 0)
+        far_weights(1, 1, True, ways=(0,))
+
+        @pl.when(z > 1)
+        def _():
+            far_weights(1, 1, True, ways=(1,))
+
         far_weights(0, planes - 1, False)
 
         @pl.when(at_end)
@@ -945,8 +959,9 @@
 
             lax.fori_loop(0, plane, last_sums, 0)
 
+
         for d in range(2, planes - 1):
-            far_weights(1, d, True, range(plane - 1))
+            far_weights(1, d, True, range(plane // 2), (1,))
 
         taps = jnp.concatenate(
             [
@@ -1076,7 +1091,8 @@
                     copy.start()
 
         for d in range(2, planes - 1):
-            far_weights(1, d, True, range(plane - 1, plane))
+            far_weights(1, d, True, range(plane // 2, plane), (1,))
+            far_weights(1, d, True, ways=(0,))
         for d in range(1, planes - 1):
             far_weights(1, d, False)
 

time: 75.7 us -> 74.7 us (0.987)
  Pallas kernels: 74.9 us -> 73.4 us
    pallas_call x1, Pallas kernels: 74 us -> 72.5 us  [fused(): pl.pallas_call(kernel, out_shape=results, in_specs=[hbm] * loaded, out_sp...]
where the time goes in v4:
time: 74.7 us; the launch traced here: 74 us
  Pallas kernels  73.4 us (98%)
    pallas_call x1, Pallas kernels, fused(): pl.pallas_call(kernel, out_shape=results, in_specs=[hbm] * loaded, out_sp...  72.5 us

profile of v4, /device:TPU:28, one launch (start us, length us, event | category | flops | bytes accessed | tf_op | source)
XLA Modules:
  0.0 74.0 jit_solution(5942803854050322616)
XLA Ops:
  0.6 72.5 %fused.1 = (bf16[256,512]{1,0:T(8,128)(2,1)S(1)}, bf16[256,1024]{1,0:T(8,128)(2,1)S(1)}) custom-call(bf16[128,1024]{1,0:T(8,128)(2,1)} %refs_0_.1, bf16[128,512]{1,0:T(8,128)(2,1)} %refs_1_.1, bf16[128,512]{1,0:T(8,128)(2,1)} %refs_2_.1, bf16[128,1024]{1,0:T(8,128)(2,1)} %refs_3_.1, bf16[128,2048]{1,0:T(8,128)(2,1)} %refs_4_.1, f32[1,2048]{1,0:T(1,128)} %bitcast.9, ...), custom_call_target="tpu_custom_call" | custom-call | tf_op jit(solution)/shard_map/fused/pallas_call | solution.py:1267
  73.1 0.9 %settle.1 = (bf16[256,512]{1,0:T(8,128)(2,1)}, bf16[256,1024]{1,0:T(8,128)(2,1)}) custom-call(bf16[256,512]{1,0:T(8,128)(2,1)S(1)} %get-tuple-element.4.a_in, bf16[256,1024]{1,0:T(8,128)(2,1)S(1)} %get-tuple-element.5.b_in), custom_call_target="tpu_custom_call" | custom-call | tf_op jit(solution)/shard_map/settle/pallas_call | solution.py:1342

commit v5 on v4

--- a/solution.py
+++ b/solution.py
@@ -1069,17 +1069,50 @@
             )
 
         def to_send(d):
-            return (z + d < planes) & ((z == 0) | (d == 1))
+            if d == 1:
+                return z + 1 < planes
+            return (z == 0) & (d + 1 < planes)
+
+        gather_all = (z > 0) & (z + 2 == planes)
+
+        def gather_states():
+            @pl.when(z == 0)
+            def _():
+                incoming[...] = jnp.zeros(incoming.shape, f32)
+
+            @pl.when(z > 0)
+            def _():
+                state_arrived(0)
+
+            @pl.when(z == 1)
+            def _():
+                incoming[...] = srecv[0].astype(f32)
+
+            @pl.when(z > 1)
+            def _():
+                incoming[...] = (
+                    per_row(jnp.exp(trecv[z - 1][:1])) * srecv[0].astype(f32)
+                    + srecv[z - 1].astype(f32)
+                )
 
         @pl.when((z > 1) & (z + 1 < planes))
         def _():
             state_arrived(z - 1)
+
+        @pl.when((z > 1) & (z + 2 < planes))
+        def _():
             ssend[...] = (
                 per_row(jnp.exp(dsum[:1])) * srecv[z - 1].astype(f32) + state[...]
             ).astype(bf16)
             tsend[...] = dsum[...] + trecv[z - 1]
 
-        @pl.when(z <= 1)
+        @pl.when(gather_all)
+        def _():
+            gather_states()
+            ssend[...] = (per_row(jnp.exp(dsum[:1])) * incoming[...] + state[...]).astype(bf16)
+            tsend[...] = dsum[...]
+
+        @pl.when((z <= 1) & jnp.logical_not(gather_all))
         def _():
             ssend[...] = state[...].astype(bf16)
             tsend[...] = dsum[...]
@@ -1104,26 +1137,36 @@
             return carry
 
         lax.fori_loop(0, plane, gate_tile, 0)
-        @pl.when((z > 1) & (z + 1 == planes))
+        @pl.when(z + 1 == planes)
         def _():
             state_arrived(z - 1)
-
-        @pl.when(z > 0)
+            incoming[...] = srecv[z - 1].astype(f32)
+
+        @pl.when((z + 1 < planes) & jnp.logical_not(gather_all))
         def _():
-            state_arrived(0)
-
-        @pl.when(z == 1)
-        def _():
-            incoming[...] = srecv[0].astype(f32)
-
-        @pl.when(z > 1)
-        def _():
-            incoming[...] = (
-                per_row(jnp.exp(trecv[z - 1][:1])) * srecv[0].astype(f32)
-                + srecv[z - 1].astype(f32)
-            )
-
-        def carry_tile(k, carry):
+            gather_states()
+
+        far_weights(1, planes - 1, False)
+        own_columns = pl.ds(pl.multiple_of(n * hw, hw), hw)
+        gain = ggain[:, own_columns]
+
+        def out_copy(k):
+            return rcopy(
+                stage.at[k], scan_out.at[:, own_columns], out_send.at[k], out_recv.at[n],
+                z * plane + k, core,
+            )
+
+        def finish(i, carry):
+            k = turned_slot(plane - 1 - i)
+
+            @pl.when(at_end)
+            def _():
+                def store(out, add):
+                    gatef[tile(k), :] = gatef[tile(k), :] + out
+
+                sum_far(1, tile(k), store)
+
+            gate = gatef[tile(k), :].astype(bf16).astype(f32)
             entered = (
                 before[k] + per_row(jnp.exp(decayed[k][:1])) * incoming[...]
             ).astype(bf16)
@@ -1131,36 +1174,7 @@
                 cbuf[tile(k), hw + ww : lower], entered, last_contract,
                 preferred_element_type=f32,
             )
-            ybuf[tile(k), :] = ybuf[tile(k), :] + carried * per_lane(jnp.exp(runs[k]))
-            return carry
-
-        @pl.when(z == 0)
-        def _():
-            incoming[...] = jnp.zeros(incoming.shape, f32)
-
-        lax.fori_loop(0, plane, carry_tile, 0)
-        far_weights(1, planes - 1, False)
-        own_columns = pl.ds(pl.multiple_of(n * hw, hw), hw)
-        gain = ggain[:, own_columns]
-
-        def out_copy(k):
-            return rcopy(
-                stage.at[k], scan_out.at[:, own_columns], out_send.at[k], out_recv.at[n],
-                z * plane + k, core,
-            )
-
-        def finish(i, carry):
-            k = turned_slot(plane - 1 - i)
-
-            @pl.when(at_end)
-            def _():
-                def store(out, add):
-                    gatef[tile(k), :] = gatef[tile(k), :] + out
-
-                sum_far(1, tile(k), store)
-
-            gate = gatef[tile(k), :].astype(bf16).astype(f32)
-            mixed = ybuf[tile(k), :]
+            mixed = ybuf[tile(k), :] + carried * per_lane(jnp.exp(runs[k]))
             gated = mixed * (gate * jax.nn.sigmoid(gate))
             out = normed_rows(gated, gain, hw).astype(bf16)
             stage[k] = out

time: 74.7 us -> 74.1 us (level)
  no operation moved by 1% of the time
where the time goes in v5:
time: 74.1 us; the launch traced here: 73.5 us
  Pallas kernels  72.9 us (98%)
    pallas_call x1, Pallas kernels, fused(): pl.pallas_call(kernel, out_shape=results, in_specs=[hbm] * loaded, out_sp...  72 us

profile of v5, /device:TPU:28, one launch (start us, length us, event | category | flops | bytes accessed | tf_op | source)
XLA Modules:
  0.0 73.5 jit_solution(268207818086313156)
XLA Ops:
  0.6 72.0 %fused.1 = (bf16[256,512]{1,0:T(8,128)(2,1)S(1)}, bf16[256,1024]{1,0:T(8,128)(2,1)S(1)}) custom-call(bf16[128,1024]{1,0:T(8,128)(2,1)} %refs_0_.1, bf16[128,512]{1,0:T(8,128)(2,1)} %refs_1_.1, bf16[128,512]{1,0:T(8,128)(2,1)} %refs_2_.1, bf16[128,1024]{1,0:T(8,128)(2,1)} %refs_3_.1, bf16[128,2048]{1,0:T(8,128)(2,1)} %refs_4_.1, f32[1,2048]{1,0:T(1,128)} %bitcast.9, ...), custom_call_target="tpu_custom_call" | custom-call | tf_op jit(solution)/shard_map/fused/pallas_call | solution.py:1281
  72.6 0.9 %settle.1 = (bf16[256,512]{1,0:T(8,128)(2,1)}, bf16[256,1024]{1,0:T(8,128)(2,1)}) custom-call(bf16[256,512]{1,0:T(8,128)(2,1)S(1)} %get-tuple-element.4.a_in, bf16[256,1024]{1,0:T(8,128)(2,1)S(1)} %get-tuple-element.5.b_in), custom_call_target="tpu_custom_call" | custom-call | tf_op jit(solution)/shard_map/settle/pallas_call | solution.py:1356
